TPU v7x, 32 devices: a whole 2x2x4 slice. The times are simulated.
32 devices in a mesh: sp: 4 (over y, x), tp: 8 (over z, core).
Axes of the slice: x: 2, y: 2, z: 4, core: 2. Of those that a mesh axis runs over, the one named last changes fastest.
Arguments:
- queries: bfloat16 [2048, 2048], P('sp', 'tp'), may hold values from -16 to 16
- key_vectors: bfloat16 [2048, 2048], P('sp', 'tp'), may hold values from -4 to 4
- value_vectors: bfloat16 [2048, 2048], P('sp', 'tp'), may hold values from -5 to 5
- forget_totals: float32 [2048, 16], P('sp', 'tp'), may hold values from -344 to 0, as said below
- head_gain: float32 [2048], P('tp'), may hold values from 0.1 to 1.9
- stream: bfloat16 [2048, 2048], P(('sp', 'tp')), may hold values from -6 to 6
- out_weight: bfloat16 [2048, 2048], replicated, may hold values from -0.125 to 0.125
- norm_gain: float32 [2048], replicated, may hold values from 0.1 to 1.9
- routing: int32 [2048, 2], P(('sp', 'tp')), may hold values from 0 to 3, all different within a row; in each aligned block of 64 rows (0 to 63, 64 to 127, ...) at most 64 rows name the same one
- route_weights: float32 [2048, 2], P(('sp', 'tp')), may hold values from 0.2 to 1
- gate_weight: bfloat16 [4, 2048, 4096], P('sp', None, 'tp'), may hold values from -0.125 to 0.125
- up_weight: bfloat16 [4, 2048, 4096], P('sp', None, 'tp'), may hold values from -0.125 to 0.125
- down_weight: bfloat16 [4, 4096, 2048], P('sp', 'tp'), may hold values from -0.09375 to 0.09375
Outputs:
- layer_out: bfloat16 [2048, 2048], P(('sp', 'tp'))
Inputs may be any that keep to these rules, and one draw needn't show every extreme that they name: `forget_totals`: along the positions, the values of each head never rise. `routing`: A token's 2 experts differ. Within the tokens of one device (aligned blocks of 64 rows) no expert is named more than 64 times.
All inputs are finite; a program needn't handle non-finite values.
Results may differ from a plain program's by a relative error of at most 0.01145.
Values may be sent and summed in bfloat16 or wider, within the bound.
A program may use at most 128 MiB of HBM per device.

v0:
```python
from functools import partial

import jax
import jax.numpy as jnp
from jax import lax
from jax.experimental import pallas as pl
from jax.experimental.pallas import tpu as pltpu
from jax.sharding import PartitionSpec as P

HD = 128
TOP = 2


masked_score = -1e30


def attend_block(
    totals, query_rows, query_gate, query_pos, key_rows, value_rows, key_gate, key_pos
):
    run_max, run_sum, run_acc = totals
    scores = jnp.einsum("qhd,khd->hqk", query_rows, key_rows, preferred_element_type=jnp.float32)
    scores = scores * HD ** (-0.5) + query_gate[:, :, None] - key_gate[:, None, :]
    visible = (key_pos[None, :] <= query_pos[:, None])[None]
    scores = jnp.where(visible, scores, masked_score)
    new_max = jnp.maximum(run_max, jnp.max(scores, axis=2))
    lifted = jnp.where(visible, jnp.exp(scores - new_max[:, :, None]), 0.0)
    rescale = jnp.exp(run_max - new_max)
    new_sum = run_sum * rescale + jnp.sum(lifted, axis=2)
    product = jnp.einsum(
        "hqk,khd->hqd", lifted.astype(jnp.bfloat16), value_rows, preferred_element_type=jnp.float32
    )
    new_acc = run_acc * rescale[:, :, None] + product
    return (new_max, new_sum, new_acc)


def keep_totals(totals_in):
    return totals_in


def make_folder(segments, gathered_gates):

    def fold_keys(state_all, key_piece, first_key):
        key_part, value_part = key_piece
        key_total = key_part.shape[0]
        block_len = min(512, key_total)
        heads_dev = segments[0][0].shape[1]
        key_part = key_part.reshape(key_total, heads_dev, HD)
        value_part = value_part.reshape(key_total, heads_dev, HD)

        def one_block(block_index, state_now):
            offset = block_index * block_len
            key_rows = lax.dynamic_slice_in_dim(key_part, offset, block_len, 0)
            value_rows = lax.dynamic_slice_in_dim(value_part, offset, block_len, 0)
            key_pos = offset + jnp.arange(block_len, dtype=jnp.int32)
            key_gate = jnp.transpose(lax.dynamic_slice_in_dim(gathered_gates, offset, block_len, 0))
            updated = []
            for segment, totals_in in zip(segments, state_now):
                query_rows, query_gate, query_pos = segment
                needed = offset <= query_pos[-1]
                advance = partial(
                    attend_block,
                    query_rows=query_rows,
                    query_gate=query_gate,
                    query_pos=query_pos,
                    key_rows=key_rows,
                    value_rows=value_rows,
                    key_gate=key_gate,
                    key_pos=key_pos,
                )
                updated.append(lax.cond(needed, advance, keep_totals, totals_in))
            return tuple(updated)

        return lax.fori_loop(0, key_total // block_len, one_block, state_all)

    return fold_keys


MESH = pl.DeviceIdType.MESH
LANES = 128
QUADS = 4


def z_steps(depth):
    steps = []
    for near in range(1, depth // 2 + 1):
        for step in (near, depth - near):
            if step not in steps:
                steps.append(step)
    return steps


def experts_kernel(
    depth,
    own_rows,
    resid,
    gate_hbm,
    up_hbm,
    down_hbm,
    out_ref,
    rows_all,
    gate_w,
    up_w,
    down_w,
    hidden,
    mine,
    theirs,
    from_core,
    from_second,
    from_first,
    from_z,
    local_sems,
    ag_send_sems,
    ag_recv_sems,
    rs_send_sems,
    core_sems,
    second_sems,
    first_sems,
    z_sems,
):
    sp = lax.axis_index("sp")
    tp = lax.axis_index("tp")
    width = resid.shape[1]
    count = resid.shape[0]
    z, core = tp // 2, tp % 2
    other = 1 - core
    x_next = sp + 1 - 2 * (sp % 2)
    y_next = (sp + 2) % 4
    first = x_next * (1 - core) + y_next * core
    second = y_next * (1 - core) + x_next * core
    far = 3 - sp
    to_core = (sp, z * 2 + other)
    to_first = (first, tp)
    to_second = (second, tp)

    def to_z(step):
        return (sp, ((z + step) % depth) * 2 + core)

    steps = z_steps(depth)
    loads = [
        pltpu.make_async_copy(own_rows, rows_all.at[core * QUADS + sp, z], local_sems.at[0]),
        pltpu.make_async_copy(gate_hbm.at[0], gate_w, local_sems.at[1]),
        pltpu.make_async_copy(up_hbm.at[0], up_w, local_sems.at[2]),
        pltpu.make_async_copy(down_hbm.at[0], down_w, local_sems.at[3]),
    ]
    for load in loads:
        load.start()

    barrier = pltpu.get_barrier_semaphore()
    peers = [to_core, to_first, to_second] + [to_z(step) for step in steps]
    for peer in peers:
        pl.semaphore_signal(barrier, inc=1, device_id=peer, device_id_type=MESH)
    pl.semaphore_wait(barrier, len(peers))

    started = []

    def spread(src, group, zz, target):
        copy = pltpu.make_async_remote_copy(
            src_ref=src,
            dst_ref=rows_all.at[group, zz],
            send_sem=ag_send_sems.at[len(started)],
            recv_sem=ag_recv_sems.at[group, zz],
            device_id=target,
            device_id_type=MESH,
        )
        copy.start()
        started.append(copy)

    def arrived(group, zz):
        slot = rows_all.at[group, zz]
        pltpu.make_async_remote_copy(
            src_ref=slot,
            dst_ref=slot,
            send_sem=ag_send_sems.at[0],
            recv_sem=ag_recv_sems.at[group, zz],
            device_id=to_core,
            device_id_type=MESH,
        ).wait_recv()

    def onward(group, zz, targets):
        arrived(group, zz)
        for target in targets:
            spread(rows_all.at[group, zz], group, zz, target)

    def from_partner(quad):
        for zz in range(depth):
            arrived(other * QUADS + quad, zz)

    def experts(group, dest, quad):
        half = 256 if gate_w.shape[1] % 256 == 0 else gate_w.shape[1]

        @pl.loop(0, gate_w.shape[1] // half)
        def _(j):
            cols = pl.ds(pl.multiple_of(j * half, half), half)
            block = rows_all[group, :, :, :width].reshape(depth * count, width)
            gate_pre = jnp.dot(block, gate_w[:, cols], preferred_element_type=jnp.float32)
            up_pre = jnp.dot(block, up_w[:, cols], preferred_element_type=jnp.float32)
            hidden[:, cols] = (gate_pre / (1.0 + jnp.exp(-gate_pre)) * up_pre).astype(jnp.bfloat16)

        pieces = rows_all[group, :, :, width:].reshape(depth * count, LANES).astype(jnp.float32)
        lane = lax.broadcasted_iota(jnp.int32, pieces.shape, 1)
        weight = jnp.sum(jnp.where(lane % QUADS == sp, pieces, 0.0), axis=1, keepdims=True)
        step = 512 if width % 512 == 0 else width

        @pl.loop(0, width // step)
        def _(j):
            cols = pl.ds(pl.multiple_of(j * step, step), step)
            product = jnp.dot(hidden[...], down_w[:, cols], preferred_element_type=jnp.float32)
            dest[quad, :, :, cols] = (
                (product * weight).astype(jnp.bfloat16).reshape(depth, count, step)
            )

    returned = []

    def send_back(src, dst, sem, target):
        copy = pltpu.make_async_remote_copy(
            src_ref=src,
            dst_ref=dst,
            send_sem=rs_send_sems.at[len(returned)],
            recv_sem=sem,
            device_id=target,
            device_id_type=MESH,
        )
        copy.start()
        returned.append(copy)

    def landed(dst, sem):
        pltpu.make_async_remote_copy(
            src_ref=dst,
            dst_ref=dst,
            send_sem=rs_send_sems.at[0],
            recv_sem=sem,
            device_id=to_core,
            device_id_type=MESH,
        ).wait_recv()

    def partner_part(quad):
        experts(other * QUADS + quad, theirs, quad)
        send_back(theirs.at[quad], from_core.at[quad], core_sems.at[quad], to_core)

    def f32(value):
        return value.astype(jnp.float32)

    own_group = core * QUADS + sp
    for target in [to_z(step) for step in steps] + [to_first, to_second, to_core]:
        spread(own_rows, own_group, z, target)
    before = None
    for step in [0] + steps + [None]:
        if step:
            onward(own_group, (z - step + depth) % depth, [to_first, to_second, to_core])
        if before is not None:
            zz = (z - before + depth) % depth
            onward(core * QUADS + first, zz, [to_second, to_core])
        before = step
    for load in loads:
        load.wait()
    order = [0] + steps
    experts(own_group, mine, sp)
    from_partner(sp)
    partner_part(sp)
    for step in order:
        onward(core * QUADS + second, (z - step + depth) % depth, [to_core])
    experts(core * QUADS + first, mine, first)
    from_partner(second)
    partner_part(second)
    experts(core * QUADS + second, mine, second)
    from_partner(first)
    partner_part(first)

    back_steps = steps + [0]

    def hand_over(quad, slot):
        landed(from_core.at[quad], core_sems.at[quad])
        mine[quad] = (f32(mine[quad]) + f32(from_core[quad])).astype(jnp.bfloat16)
        for step in back_steps:
            zz = (z + step) % depth
            send_back(
                mine.at[quad, zz], from_second.at[slot, zz], second_sems.at[slot, zz], to_second
            )

    hand_over(second, 0)
    for step in order:
        onward(core * QUADS + far, (z - step + depth) % depth, [to_core])
    experts(core * QUADS + far, mine, far)
    from_partner(far)
    partner_part(far)
    hand_over(far, 1)

    landed(from_core.at[first], core_sems.at[first])
    landed(from_core.at[sp], core_sems.at[sp])
    for step in back_steps:
        zz = (z + step) % depth
        landed(from_second.at[1, zz], second_sems.at[1, zz])
        mine[first, zz] = (
            f32(mine[first, zz]) + f32(from_core[first, zz]) + f32(from_second[1, zz])
        ).astype(jnp.bfloat16)
        send_back(mine.at[first, zz], from_first.at[zz], first_sems.at[zz], to_first)
    for step in back_steps:
        zz = (z + step) % depth
        landed(from_second.at[0, zz], second_sems.at[0, zz])
        landed(from_first.at[zz], first_sems.at[zz])
        total = (
            f32(mine[sp, zz])
            + f32(from_core[sp, zz])
            + f32(from_second[0, zz])
            + f32(from_first[zz])
        )
        if step:
            mine[sp, zz] = total.astype(jnp.bfloat16)
            send_back(mine.at[sp, zz], from_z.at[step - 1], z_sems.at[step - 1], to_z(step))
        else:
            total = resid[...] + total
            for slot in range(depth - 1):
                landed(from_z.at[slot], z_sems.at[slot])
                total = total + f32(from_z[slot])
            out_ref[...] = total.astype(out_ref.dtype)
    for copy in started + returned:
        copy.wait_send()


def heads_kernel(
    queries,
    keys,
    values,
    key_gates,
    query_gates,
    gain,
    stream,
    out_hbm,
    norm_gain,
    pieces,
    resid_out,
    rows_out,
    key_all,
    value_all,
    gate_all,
    peak,
    weight_total,
    weighted,
    leaving,
    incoming,
    out_w,
    local_sem,
    kv_send_sems,
    kv_recv_sems,
    out_send_sems,
    out_recv_sems,
):
    sp = lax.axis_index("sp")
    tp = lax.axis_index("tp")
    tp_count = lax.axis_size("tp")
    tokens = queries.shape[0]
    heads = queries.shape[1] // HD
    width = resid_out.shape[1]
    count = resid_out.shape[0]
    core = tp % 2
    x_next = sp + 1 - 2 * (sp % 2)
    y_next = (sp + 2) % 4
    first = x_next * (1 - core) + y_next * core
    second = y_next * (1 - core) + x_next * core
    far = 3 - sp
    load = pltpu.make_async_copy(out_hbm, out_w, local_sem.at[0])
    load.start()

    barrier = pltpu.get_barrier_semaphore()
    peers = [(first, tp), (second, tp)]
    peers += [(sp, (tp + step) % tp_count) for step in range(1, tp_count)]
    for peer in peers:
        pl.semaphore_signal(barrier, inc=1, device_id=peer, device_id_type=MESH)
    pl.semaphore_wait(barrier, len(peers))

    started = []

    def send_block(refs, quad, target):
        for part, (src, dst) in enumerate(zip(refs, (key_all, value_all, gate_all))):
            copy = pltpu.make_async_remote_copy(
                src_ref=src,
                dst_ref=dst.at[quad],
                send_sem=kv_send_sems.at[len(started)],
                recv_sem=kv_recv_sems.at[quad, part],
                device_id=target,
                device_id_type=MESH,
            )
            copy.start()
            started.append(copy)

    def block_of(quad):
        return (key_all.at[quad], value_all.at[quad], gate_all.at[quad])

    def receive_block(quad):
        for part, ref in enumerate(block_of(quad)):
            pltpu.make_async_remote_copy(
                src_ref=ref,
                dst_ref=ref,
                send_sem=kv_send_sems.at[0],
                recv_sem=kv_recv_sems.at[quad, part],
                device_id=(first, tp),
                device_id_type=MESH,
            ).wait_recv()

    chunk = 128

    def attend(refs, diagonal):
        key_ref, value_ref, gate_ref = refs

        @pl.loop(0, tokens // chunk)
        def _(j):
            rows = pl.ds(pl.multiple_of(j * chunk, chunk), chunk)
            for head in range(heads):
                cols = slice(head * HD, (head + 1) * HD)
                scores = lax.dot_general(
                    queries[rows, cols],
                    key_ref[:, cols],
                    (((1,), (1,)), ((), ())),
                    preferred_element_type=jnp.float32,
                )
                scores = (
                    scores * HD ** (-0.5)
                    + query_gates[rows, head : head + 1]
                    - gate_ref[head : head + 1, :]
                )
                if diagonal:
                    row_id = lax.broadcasted_iota(jnp.int32, scores.shape, 0) + j * chunk
                    col_id = lax.broadcasted_iota(jnp.int32, scores.shape, 1)
                    scores = jnp.where(col_id <= row_id, scores, masked_score)
                new_peak = jnp.max(scores, axis=1, keepdims=True)
                if not diagonal:
                    old_peak = peak[head, rows]
                    new_peak = jnp.maximum(old_peak, new_peak)
                lifted = jnp.exp(scores - new_peak)
                added = jnp.sum(lifted, axis=1, keepdims=True)
                product = jnp.dot(
                    lifted.astype(jnp.bfloat16),
                    value_ref[:, cols],
                    preferred_element_type=jnp.float32,
                )
                if not diagonal:
                    rescale = jnp.exp(old_peak - new_peak)
                    added = weight_total[head, rows] * rescale + added
                    product = weighted[head, rows] * rescale + product
                peak[head, rows] = new_peak
                weight_total[head, rows] = added
                weighted[head, rows] = product

    def attend_earlier(quad):
        @pl.when(quad < sp)
        def _():
            attend(block_of(quad), False)

    own = (keys, values, key_gates)
    send_block(own, sp, (first, tp))
    send_block(own, sp, (second, tp))
    attend(own, True)
    receive_block(first)
    send_block(block_of(first), first, (second, tp))
    attend_earlier(first)
    receive_block(second)
    attend_earlier(second)
    receive_block(far)
    attend_earlier(far)

    @pl.loop(0, tp_count)
    def _(j):
        rows = pl.ds(pl.multiple_of(j * count, count), count)
        for head in range(heads):
            cols = slice(head * HD, (head + 1) * HD)
            attended = weighted[head, rows] / weight_total[head, rows]
            square = jnp.mean(attended * attended, axis=1, keepdims=True)
            normed = attended * lax.rsqrt(square + 1e-06) * gain[0:1, cols]
            leaving[j, :, cols] = normed.astype(jnp.bfloat16)

    sent = []
    for step in range(1, tp_count):
        target = (tp + step) % tp_count
        copy = pltpu.make_async_remote_copy(
            src_ref=leaving.at[target],
            dst_ref=incoming.at[tp],
            send_sem=out_send_sems.at[step],
            recv_sem=out_recv_sems.at[tp],
            device_id=(sp, target),
            device_id_type=MESH,
        )
        copy.start()
        sent.append(copy)
    resid_out[...] = stream[...].astype(jnp.float32)
    load.wait()
    wide = heads * HD
    strip = 512 if width % 512 == 0 else width
    for step in range(tp_count):
        source = (tp - step + tp_count) % tp_count
        part = leaving if step == 0 else incoming
        if step:
            slot = incoming.at[source]
            pltpu.make_async_remote_copy(
                src_ref=slot,
                dst_ref=slot,
                send_sem=out_send_sems.at[0],
                recv_sem=out_recv_sems.at[source],
                device_id=(first, tp),
                device_id_type=MESH,
            ).wait_recv()

        @pl.loop(0, width // strip)
        def _(j):
            cols = pl.ds(pl.multiple_of(j * strip, strip), strip)
            weights = out_w[pl.ds(pl.multiple_of(source * wide, wide), wide), cols]
            resid_out[:, cols] += jnp.dot(
                part[source], weights, preferred_element_type=jnp.float32
            )

    resid = resid_out[...]
    center = resid - jnp.mean(resid, axis=1, keepdims=True)
    variance = jnp.mean(center * center, axis=1, keepdims=True)
    rows_out[:, :width] = (center * lax.rsqrt(variance + 1e-05) * norm_gain[0:1, :]).astype(
        jnp.bfloat16
    )
    rows_out[:, width:] = pieces[...]
    for copy in started + sent:
        copy.wait_send()


def weight_pieces(routing, route_weights):
    experts = jnp.arange(QUADS, dtype=jnp.int32)
    named = routing[:, :, None] == experts[None, None, :]
    weights = jnp.sum(jnp.where(named, route_weights[:, :, None], 0.0), axis=1)
    high = lax.reduce_precision(weights, 8, 7)
    middle = lax.reduce_precision(weights - high, 8, 7)
    low = weights - high - middle
    pieces = jnp.concatenate([high, middle, low], axis=1).astype(jnp.bfloat16)
    return jnp.pad(pieces, ((0, 0), (0, LANES - pieces.shape[1])))


def heads_stage(
    queries, keys, values, forget_totals, head_gain, stream, out_weight, norm_gain, pieces
):
    tokens, wide = queries.shape
    heads = wide // HD
    count, width = stream.shape
    tp_count = lax.axis_size("tp")
    key_gates = jnp.pad(jnp.transpose(forget_totals), ((0, (-heads) % 8), (0, 0)))
    bf16, f32 = jnp.bfloat16, jnp.float32
    dma = pltpu.SemaphoreType.DMA
    vmem = pl.BlockSpec(memory_space=pltpu.VMEM)
    hbm = pl.BlockSpec(memory_space=pl.ANY)
    return pl.pallas_call(
        heads_kernel,
        out_shape=(
            jax.ShapeDtypeStruct((count, width), f32),
            jax.ShapeDtypeStruct((count, width + LANES), bf16),
        ),
        in_specs=[vmem] * 7 + [hbm] + [vmem] * 2,
        out_specs=(vmem, vmem),
        scratch_shapes=[
            pltpu.VMEM((QUADS, tokens, wide), bf16),
            pltpu.VMEM((QUADS, tokens, wide), bf16),
            pltpu.VMEM((QUADS,) + key_gates.shape, f32),
            pltpu.VMEM((heads, tokens, 1), f32),
            pltpu.VMEM((heads, tokens, 1), f32),
            pltpu.VMEM((heads, tokens, HD), f32),
            pltpu.VMEM((tp_count, count, wide), bf16),
            pltpu.VMEM((tp_count, count, wide), bf16),
            pltpu.VMEM(out_weight.shape, bf16),
            dma((1,)),
            dma((9,)),
            dma((QUADS, 3)),
            dma((tp_count,)),
            dma((tp_count,)),
        ],
        compiler_params=pltpu.CompilerParams(
            collective_id=1, has_side_effects=True, vmem_limit_bytes=40 * 2**20
        ),
    )(
        queries,
        keys,
        values,
        key_gates,
        forget_totals,
        head_gain.reshape(1, -1),
        stream,
        out_weight,
        norm_gain.reshape(1, -1),
        pieces,
    )


def dense_experts(resid_sum, extended, gate_weight, up_weight, down_weight):
    depth = lax.axis_size("tp") // 2
    count, width = resid_sum.shape
    units = gate_weight.shape[2]
    bf16 = jnp.bfloat16
    dma = pltpu.SemaphoreType.DMA
    block = (depth, count, width)
    vmem = pl.BlockSpec(memory_space=pltpu.VMEM)
    hbm = pl.BlockSpec(memory_space=pl.ANY)
    ag_sends = (depth - 1 + 3) + 3 * (depth - 1) + 2 * depth + 2 * depth
    rs_sends = QUADS + 2 * depth + depth + depth - 1
    return pl.pallas_call(
        partial(experts_kernel, depth),
        out_shape=jax.ShapeDtypeStruct((count, width), bf16),
        in_specs=[vmem, vmem, hbm, hbm, hbm],
        out_specs=vmem,
        scratch_shapes=[
            pltpu.VMEM((2 * QUADS, depth, count, width + LANES), bf16),
            pltpu.VMEM((width, units), bf16),
            pltpu.VMEM((width, units), bf16),
            pltpu.VMEM((units, width), bf16),
            pltpu.VMEM((depth * count, units), bf16),
            pltpu.VMEM((QUADS,) + block, bf16),
            pltpu.VMEM((QUADS,) + block, bf16),
            pltpu.VMEM((QUADS,) + block, bf16),
            pltpu.VMEM((2,) + block, bf16),
            pltpu.VMEM(block, bf16),
            pltpu.VMEM((depth - 1, count, width), bf16),
            dma((4,)),
            dma((ag_sends,)),
            dma((2 * QUADS, depth)),
            dma((rs_sends,)),
            dma((QUADS,)),
            dma((2, depth)),
            dma((depth,)),
            dma((depth - 1,)),
        ],
        compiler_params=pltpu.CompilerParams(
            collective_id=0, has_side_effects=True, vmem_limit_bytes=48 * 2**20
        ),
    )(extended, resid_sum, gate_weight, up_weight, down_weight)


def routed_experts(
    resid_sum, normed_rows, routing, route_weights, gate_weight, up_weight, down_weight
):
    sp_count = lax.axis_size("sp")
    row_count = normed_rows.shape[0]
    capacity = max(2, 2 * TOP * row_count // sp_count)
    flat_expert = routing.reshape(-1)
    onehot = (flat_expert[:, None] == jnp.arange(sp_count, dtype=jnp.int32)[None, :]).astype(
        jnp.int32
    )
    earlier = jnp.cumsum(onehot, axis=0) - onehot
    slot_index = flat_expert * capacity + jnp.sum(earlier * onehot, axis=1)
    slot_grid = slot_index.reshape(row_count, TOP)
    slot_ids = jnp.arange(sp_count * capacity, dtype=jnp.int32)
    placing = jnp.sum(
        (slot_grid[None, :, :] == slot_ids[:, None, None]).astype(jnp.float32), axis=2
    ).astype(jnp.bfloat16)
    outgoing = jnp.dot(placing, normed_rows, preferred_element_type=jnp.float32).astype(
        jnp.bfloat16
    )
    outgoing = outgoing.reshape(sp_count, capacity, normed_rows.shape[1])
    arrived = lax.all_to_all(outgoing, "sp", split_axis=0, concat_axis=0, tiled=True)
    row_piece = lax.all_gather(arrived.reshape(-1, arrived.shape[2]), "tp", axis=0, tiled=True)
    gate_pre = jnp.dot(row_piece, gate_weight[0], preferred_element_type=jnp.float32)
    up_pre = jnp.dot(row_piece, up_weight[0], preferred_element_type=jnp.float32)
    hidden = (jax.nn.silu(gate_pre) * up_pre).astype(jnp.bfloat16)
    summed = lax.psum_scatter(
        jnp.dot(hidden, down_weight[0], preferred_element_type=jnp.float32).astype(jnp.bfloat16),
        "tp",
        scatter_dimension=0,
        tiled=True,
    )
    expert_out = summed.reshape(sp_count, capacity, -1)
    returned = lax.all_to_all(expert_out, "sp", split_axis=0, concat_axis=0, tiled=True)
    picked = returned.reshape(sp_count * capacity, -1)[slot_index].astype(jnp.float32)
    weighted = picked * route_weights.reshape(-1)[:, None]
    routed = jnp.sum(weighted.reshape(row_count, TOP, -1), axis=1)
    return (resid_sum + routed).astype(jnp.bfloat16)


def on_device(
    queries,
    key_vectors,
    value_vectors,
    forget_totals,
    head_gain,
    stream,
    out_weight,
    norm_gain,
    routing,
    route_weights,
    gate_weight,
    up_weight,
    down_weight,
):
    rows_dev, sp_size, tp_size = stream.shape[0], lax.axis_size("sp"), lax.axis_size("tp")
    dense = 2 * TOP * rows_dev // sp_size >= rows_dev
    if dense and sp_size == QUADS and tp_size % 4 == 0 and queries.shape[0] % 128 == 0:
        resid_sum, extended = heads_stage(
            queries,
            key_vectors,
            value_vectors,
            forget_totals,
            head_gain,
            stream,
            out_weight,
            norm_gain,
            weight_pieces(routing, route_weights),
        )
        return dense_experts(resid_sum, extended, gate_weight, up_weight, down_weight)
    tok_count = queries.shape[0]
    heads_dev = queries.shape[1] // HD
    sp_index = lax.axis_index("sp")
    sp_count = lax.axis_size("sp")
    gathered_gates = lax.all_gather(forget_totals, "sp", axis=0, tiled=True)
    first_pos = sp_index * tok_count
    query_pos = first_pos + jnp.arange(tok_count, dtype=jnp.int32)
    query_gate = jnp.transpose(lax.dynamic_slice_in_dim(gathered_gates, first_pos, tok_count, 0))
    segments = [(queries.reshape(tok_count, heads_dev, HD), query_gate, query_pos)]
    starting = (
        (
            jnp.full((heads_dev, tok_count), masked_score, jnp.float32),
            jnp.zeros((heads_dev, tok_count), jnp.float32),
            jnp.zeros((heads_dev, tok_count, HD), jnp.float32),
        ),
    )
    folder = make_folder(segments, gathered_gates)
    totals = folder(
        starting,
        (
            lax.all_gather(key_vectors, "sp", axis=0, tiled=True),
            lax.all_gather(value_vectors, "sp", axis=0, tiled=True),
        ),
        jnp.int32(0),
    )
    run_max, run_sum, run_acc = totals[0]
    attended = run_acc / run_sum[:, :, None]
    inverse_rms = lax.rsqrt(jnp.mean(attended * attended, axis=2, keepdims=True) + 1e-06)
    normed = attended * inverse_rms * head_gain.reshape(heads_dev, 1, HD)
    head_out = (
        jnp.transpose(normed, (1, 0, 2)).reshape(tok_count, heads_dev * HD).astype(jnp.bfloat16)
    )
    token_heads = lax.all_to_all(head_out, "tp", split_axis=0, concat_axis=1, tiled=True)
    mixed_rows = jnp.dot(token_heads, out_weight, preferred_element_type=jnp.float32)
    resid_sum = stream.astype(jnp.float32) + mixed_rows
    center = resid_sum - jnp.mean(resid_sum, axis=1, keepdims=True)
    normed_rows = (
        center * lax.rsqrt(jnp.mean(center * center, axis=1, keepdims=True) + 1e-05) * norm_gain
    ).astype(jnp.bfloat16)
    return routed_experts(
        resid_sum, normed_rows, routing, route_weights, gate_weight, up_weight, down_weight
    )


def solution(mesh):
    in_specs = (
        P("sp", "tp"),
        P("sp", "tp"),
        P("sp", "tp"),
        P("sp", "tp"),
        P("tp"),
        P(("sp", "tp"), None),
        P(),
        P(),
        P(("sp", "tp"), None),
        P(("sp", "tp"), None),
        P("sp", None, "tp"),
        P("sp", None, "tp"),
        P("sp", "tp", None),
    )
    out_specs = P(("sp", "tp"), None)
    return jax.shard_map(
        on_device, mesh=mesh, in_specs=in_specs, out_specs=out_specs, check_vma=False
    )
```

profile of v0, /device:TPU:0, one launch (start us, length us, event | category | flops | bytes accessed | tf_op | source)
XLA Modules:
  0.0 163.2 jit_solution(8861205480778801418)
XLA Ops:
  0.0 0.7 select_reduce_fusion
  0.7 0.1 copy.21
  0.9 0.7 pad.8.key_gates
  1.5 0.8 copy.22.query_gates
  2.4 0.0 copy-start
  2.4 3.4 %copy-done = bf16[2048,2048]{1,0:T(8,128)(2,1)S(1)} copy-done((bf16[2048,2048]{1,0:T(8,128)(2,1)S(1)}, bf16[2048,2048]{1,0:T(8,128)(2,1)}, u32[]{:S(2)}) %copy-start) | copy-done | bytes 8388632
  5.8 0.0 copy-start.3
  5.8 0.9 copy-done.3
  6.7 0.0 copy-start.4
  6.7 0.9 copy-done.4
  7.7 0.0 copy-start.5
  7.7 0.9 copy-done.5
  8.6 0.0 copy-start.6
  8.6 0.9 copy-done.6
  9.6 0.0 copy-start.7
  9.6 0.7 copy-done.7
  10.3 0.0 copy-start.8
  10.3 0.7 copy-done.8
  10.9 0.0 copy-start.1
  11.0 37.6 %shard_map.127 = (f32[64,2048]{1,0:T(8,128)S(1)}, bf16[64,2176]{1,0:T(8,128)(2,1)S(1)}) custom-call(bf16[512,256]{1,0:T(8,128)(2,1)S(1)} %copy-done.3, bf16[512,256]{1,0:T(8,128)(2,1)S(1)} %copy-done.4, bf16[512,256]{1,0:T(8,128)(2,1)S(1)} %copy-done.5, f32[8,512]{1,0:T(8,128)S(1)} %pad.8.key_gates, f32[512,2]{1,0:T(8,128)S(1)} %copy.22.query_gates, ...), custom_call_target="tpu_custom_call" | custom-call | tf_op jit(solution)/shard_map/pallas_call | solution.py:544
  48.5 0.0 copy-done.1
  48.5 0.0 copy-done.2
  48.5 114.0 %shard_map.128 = bf16[64,2048]{1,0:T(8,128)(2,1)S(1)} custom-call(bf16[64,2176]{1,0:T(8,128)(2,1)S(1)} %get-tuple-element.7.own_rows, f32[64,2048]{1,0:T(8,128)S(1)} %get-tuple-element.8.resid, bf16[1,2048,512]{2,1,0:T(8,128)(2,1)S(1)} %copy-done.1, bf16[1,2048,512]{2,1,0:T(8,128)(2,1)S(1)} %copy-done.2, bf16[1,512,2048]{2,1,0:T(8,128)(2,1)} %down_hbm.1), custom_call_target="tpu_custom_call" | custom-call | tf_op jit(solution)/shard_map/pallas_call | solution.py:596
  162.5 0.7 copy.24
  (4 shorter events, 0.0 us)
Async XLA Ops:
  2.4 3.4 %copy-start = (bf16[2048,2048]{1,0:T(8,128)(2,1)S(1)}, bf16[2048,2048]{1,0:T(8,128)(2,1)}, u32[]{:S(2)}) copy-start(bf16[2048,2048]{1,0:T(8,128)(2,1)} %out_hbm.1) | copy-start | bytes 25165828
  5.8 0.9 copy-start.3
  6.7 0.9 copy-start.4
  7.7 0.9 copy-start.5
  8.6 0.9 copy-start.6
  9.6 0.7 copy-start.7
  10.3 0.7 copy-start.8
  10.9 37.6 %copy-start.1 = (bf16[1,2048,512]{2,1,0:T(8,128)(2,1)S(1)}, bf16[1,2048,512]{2,1,0:T(8,128)(2,1)}, u32[]{:S(2)}) copy-start(bf16[1,2048,512]{2,1,0:T(8,128)(2,1)} %gate_hbm.1) | copy-start | bytes 6291460
  11.0 37.6 %copy-start.2 = (bf16[1,2048,512]{2,1,0:T(8,128)(2,1)S(1)}, bf16[1,2048,512]{2,1,0:T(8,128)(2,1)}, u32[]{:S(2)}) copy-start(bf16[1,2048,512]{2,1,0:T(8,128)(2,1)} %up_hbm.1) | copy-start | bytes 6291460
where the time goes:
time: 164 us; the launch traced here: 163 us
  Pallas kernels  152 us (93%)
  local copies, waits for them, and re-layouts  10.9 us (7%)
    pallas_call x1, Pallas kernels, dense_experts(): pl.pallas_call(partial(experts_kernel, depth), out_shape=jax.ShapeDtypeSt...  114 us
    pallas_call x1, Pallas kernels, heads_stage(): pl.pallas_call(heads_kernel, out_shape=(jax.ShapeDtypeStruct((count, widt...  37.6 us
    unnamed x20, local copies, waits for them, and re-layouts  10.1 us

commit v1 on v0

v1 whole, which is shorter than its diff:
```python
from functools import partial

import jax
import jax.numpy as jnp
from jax import lax
from jax.experimental import pallas as pl
from jax.experimental.pallas import tpu as pltpu
from jax.sharding import PartitionSpec as P

HD = 128
TOP = 2


masked_score = -1e30


def attend_block(
    totals, query_rows, query_gate, query_pos, key_rows, value_rows, key_gate, key_pos
):
    run_max, run_sum, run_acc = totals
    scores = jnp.einsum("qhd,khd->hqk", query_rows, key_rows, preferred_element_type=jnp.float32)
    scores = scores * HD ** (-0.5) + query_gate[:, :, None] - key_gate[:, None, :]
    visible = (key_pos[None, :] <= query_pos[:, None])[None]
    scores = jnp.where(visible, scores, masked_score)
    new_max = jnp.maximum(run_max, jnp.max(scores, axis=2))
    lifted = jnp.where(visible, jnp.exp(scores - new_max[:, :, None]), 0.0)
    rescale = jnp.exp(run_max - new_max)
    new_sum = run_sum * rescale + jnp.sum(lifted, axis=2)
    product = jnp.einsum(
        "hqk,khd->hqd", lifted.astype(jnp.bfloat16), value_rows, preferred_element_type=jnp.float32
    )
    new_acc = run_acc * rescale[:, :, None] + product
    return (new_max, new_sum, new_acc)


def keep_totals(totals_in):
    return totals_in


def make_folder(segments, gathered_gates):

    def fold_keys(state_all, key_piece, first_key):
        key_part, value_part = key_piece
        key_total = key_part.shape[0]
        block_len = min(512, key_total)
        heads_dev = segments[0][0].shape[1]
        key_part = key_part.reshape(key_total, heads_dev, HD)
        value_part = value_part.reshape(key_total, heads_dev, HD)

        def one_block(block_index, state_now):
            offset = block_index * block_len
            key_rows = lax.dynamic_slice_in_dim(key_part, offset, block_len, 0)
            value_rows = lax.dynamic_slice_in_dim(value_part, offset, block_len, 0)
            key_pos = offset + jnp.arange(block_len, dtype=jnp.int32)
            key_gate = jnp.transpose(lax.dynamic_slice_in_dim(gathered_gates, offset, block_len, 0))
            updated = []
            for segment, totals_in in zip(segments, state_now):
                query_rows, query_gate, query_pos = segment
                needed = offset <= query_pos[-1]
                advance = partial(
                    attend_block,
                    query_rows=query_rows,
                    query_gate=query_gate,
                    query_pos=query_pos,
                    key_rows=key_rows,
                    value_rows=value_rows,
                    key_gate=key_gate,
                    key_pos=key_pos,
                )
                updated.append(lax.cond(needed, advance, keep_totals, totals_in))
            return tuple(updated)

        return lax.fori_loop(0, key_total // block_len, one_block, state_all)

    return fold_keys


MESH = pl.DeviceIdType.MESH
LANES = 128
QUADS = 4
LOG2E = 1.4426950408889634

TASKS = (
    ("far", 0),
    ("zar", 1),
    ("zar", 2),
    ("s", 0),
    ("f", 0),
    ("far", 1),
    ("co", 0),
    ("zar", 3),
    ("cp", 0),
    ("far", 2),
    ("s", 1),
    ("f", 1),
    ("co", 1),
    ("far", 3),
    ("r1", 0),
    ("cp", 1),
    ("s", 2),
    ("f", 2),
    ("co", 2),
    ("r1", 1),
    ("cp", 2),
    ("r1", 2),
    ("s", 3),
    ("f", 3),
    ("co", 3),
    ("cp", 3),
    ("r2", 1),
    ("r3", 1),
    ("r1", 3),
    ("r2", 2),
    ("r3", 2),
    ("r2", 3),
    ("r3", 3),
    ("r2", 0),
    ("r3", 0),
)


def layer_kernel(
    depth,
    queries_hbm,
    keys_hbm,
    values_hbm,
    gates_hbm,
    gain_hbm,
    stream_hbm,
    out_hbm,
    norm_hbm,
    routing_hbm,
    route_hbm,
    gate_hbm,
    up_hbm,
    down_hbm,
    out_ref,
    queries,
    stream,
    gain,
    norm_gain,
    routing,
    route_w,
    key_all,
    value_all,
    gate_all,
    weights_all,
    wcols,
    qcol,
    peak,
    weight_total,
    weighted,
    leaving,
    incoming,
    resid,
    out_w,
    rows_all,
    gate_w,
    up_w,
    down_w,
    hidden,
    mine,
    theirs,
    from_core,
    from_second,
    from_first,
    from_z,
    from_zf,
    local_sems,
    kv_send_sems,
    kv_recv_sems,
    out_send_sems,
    out_recv_sems,
    w_send_sems,
    w_recv_sems,
    wq_recv_sems,
    ag_send_sems,
    ag_recv_sems,
    rs_send_sems,
    core_sems,
    second_sems,
    first_sems,
    z_sems,
    zf_sems,
):
    sp = lax.axis_index("sp")
    tp = lax.axis_index("tp")
    tp_count = 2 * depth
    tokens = queries.shape[0]
    heads = queries.shape[1] // HD
    count, width = resid.shape
    units = gate_w.shape[1]
    z, core = tp // 2, tp % 2
    other = 1 - core
    x_next = sp + 1 - 2 * (sp % 2)
    y_next = (sp + 2) % 4
    first = x_next * (1 - core) + y_next * core
    second = y_next * (1 - core) + x_next * core
    far = 3 - sp
    to_core = (sp, z * 2 + other)
    to_first = (first, tp)
    to_second = (second, tp)

    def f32(value):
        return value.astype(jnp.float32)

    def bf16(value):
        return value.astype(jnp.bfloat16)

    def at_z(level):
        return (sp, level * 2 + core)

    orders = []
    for at in range(depth):
        order = [at]
        for step in range(1, depth):
            order += [lev for lev in (at - step, at + step) if 0 <= lev < depth]
        orders.append(order)
    levels = []
    for place in range(depth):
        total = 0
        for at in range(depth):
            apart = (z - at + depth) % depth
            total = total + orders[at][place] * (1 - (apart + depth - 1) // depth)
        levels.append(total)

    def adjacent(level):
        return (level - z) * (level - z) == 1

    loads = {}

    def load(name, src, dst):
        loads[name] = pltpu.make_async_copy(src, dst, local_sems.at[len(loads)])
        loads[name].start()

    load("keys", keys_hbm, key_all.at[sp])
    load("values", values_hbm, value_all.at[sp])
    load("gates", gates_hbm, gate_all.at[sp])
    load("queries", queries_hbm, queries)
    load("routing", routing_hbm, routing)
    load("route", route_hbm, route_w)

    barrier = pltpu.get_barrier_semaphore()
    peers = [to_first, to_second]
    peers += [(sp, (tp + step) % tp_count) for step in range(1, tp_count)]
    for peer in peers:
        pl.semaphore_signal(barrier, inc=1, device_id=peer, device_id_type=MESH)
    pl.semaphore_wait(barrier, len(peers))

    sent = []

    def send(src, dst, send_sem, recv_sem, target, when=None):
        copy = pltpu.make_async_remote_copy(
            src_ref=src,
            dst_ref=dst,
            send_sem=send_sem,
            recv_sem=recv_sem,
            device_id=target,
            device_id_type=MESH,
        )
        if when is None:
            copy.start()
        else:
            pl.when(when)(copy.start)
        sent.append((copy, when))

    def landed(dst, sem):
        pltpu.make_async_remote_copy(
            src_ref=dst,
            dst_ref=dst,
            send_sem=kv_send_sems.at[0],
            recv_sem=sem,
            device_id=to_core,
            device_id_type=MESH,
        ).wait_recv()

    kv_refs = (key_all, value_all, gate_all)
    kv_count = [0]

    def kv_send(quad, part, target):
        ref = kv_refs[part].at[quad]
        send(ref, ref, kv_send_sems.at[kv_count[0]], kv_recv_sems.at[quad, part], target)
        kv_count[0] += 1

    def kv_landed(quad, part):
        landed(kv_refs[part].at[quad], kv_recv_sems.at[quad, part])

    for part, name in enumerate(("keys", "values", "gates")):
        loads[name].wait()
        kv_send(sp, part, to_first)
        kv_send(sp, part, to_second)
    load("stream", stream_hbm, stream)
    load("gain", gain_hbm, gain)
    load("norm", norm_hbm, norm_gain)
    load("out", out_hbm, out_w)
    load("gate", gate_hbm.at[0], gate_w)
    load("up", up_hbm.at[0], up_w)
    load("down", down_hbm.at[0], down_w)

    for name in ("routing", "route", "queries"):
        loads[name].wait()
    own_weights = weights_all.at[sp, tp]
    own_weights[...] = jnp.zeros_like(own_weights)
    for expert in range(QUADS):
        row = 0.0
        for k in range(routing.shape[0]):
            row = row + jnp.where(
                routing[k : k + 1, :] == expert, route_w[k : k + 1, :], 0.0
            )
        own_weights[expert : expert + 1, :count] = row

    chunk = LANES
    for head in range(heads):
        for at in range(tokens // chunk):
            span = slice(at * chunk, (at + 1) * chunk)
            row = gate_all[sp, head : head + 1, span] * LOG2E
            qcol[head, span] = jnp.transpose(jnp.broadcast_to(row, (chunk, chunk)))[:, :1]

    def attend(quad, diagonal):
        @pl.loop(0, tokens // chunk)
        def _(j):
            rows = pl.ds(pl.multiple_of(j * chunk, chunk), chunk)
            for head in range(heads):
                cols = slice(head * HD, (head + 1) * HD)
                scores = lax.dot_general(
                    queries[rows, cols],
                    key_all[quad, :, cols],
                    (((1,), (1,)), ((), ())),
                    preferred_element_type=jnp.float32,
                )
                query_gate = qcol[head, rows]
                key_gate = gate_all[quad, head : head + 1, :] * LOG2E
                scores = scores * (HD ** (-0.5) * LOG2E) - key_gate
                if diagonal:
                    row_id = lax.broadcasted_iota(jnp.int32, scores.shape, 0) + j * chunk
                    col_id = lax.broadcasted_iota(jnp.int32, scores.shape, 1)
                    scores = jnp.where(col_id <= row_id, scores, masked_score)
                new_peak = jnp.max(scores, axis=1, keepdims=True) + query_gate
                if not diagonal:
                    old_peak = peak[head, rows]
                    new_peak = jnp.maximum(old_peak, new_peak)
                lifted = jnp.exp2(scores + (query_gate - new_peak))
                added = jnp.sum(lifted, axis=1, keepdims=True)
                product = jnp.dot(
                    lifted.astype(jnp.bfloat16),
                    value_all[quad, :, cols],
                    preferred_element_type=jnp.float32,
                )
                if not diagonal:
                    rescale = jnp.exp2(old_peak - new_peak)
                    added = weight_total[head, rows] * rescale + added
                    product = weighted[head, rows] * rescale + product
                peak[head, rows] = new_peak
                weight_total[head, rows] = added
                weighted[head, rows] = product

    def attend_earlier(quad):
        @pl.when(quad < sp)
        def _():
            attend(quad, False)

    attend(sp, True)
    for step in range(1, tp_count):
        target = (tp + step) % tp_count
        ref = weights_all.at[sp, tp]
        send(ref, ref, w_send_sems.at[step], w_recv_sems.at[tp], (sp, target))
    for part in range(3):
        kv_landed(first, part)
        kv_send(first, part, to_second)
    attend_earlier(first)
    for part in range(3):
        kv_landed(second, part)
    attend_earlier(second)
    for step in range(1, tp_count):
        source = (tp + step) % tp_count
        landed(weights_all.at[sp, source], w_recv_sems.at[source])
    for part in range(3):
        kv_landed(far, part)
    attend_earlier(far)

    loads["gain"].wait()

    @pl.loop(0, tp_count)
    def _(j):
        rows = pl.ds(pl.multiple_of(j * count, count), count)
        for head in range(heads):
            cols = slice(head * HD, (head + 1) * HD)
            attended = weighted[head, rows] / weight_total[head, rows]
            square = jnp.mean(attended * attended, axis=1, keepdims=True)
            normed = attended * lax.rsqrt(square + 1e-06) * gain[0:1, cols]
            leaving[j, :, cols] = normed.astype(jnp.bfloat16)

    for at, level in enumerate(reversed(levels)):
        for side in (core, other):
            if at == depth - 1 and side is core:
                continue
            target = level * 2 + side
            index = 2 * at + (0 if side is core else 1)
            send(
                leaving.at[target],
                incoming.at[tp],
                out_send_sems.at[index],
                out_recv_sems.at[tp],
                (sp, target),
            )

    send(weights_all.at[sp], weights_all.at[sp], w_send_sems.at[0], wq_recv_sems.at[sp], to_first)
    send(
        weights_all.at[sp],
        weights_all.at[sp],
        w_send_sems.at[tp_count],
        wq_recv_sems.at[sp],
        to_second,
    )
    loads["stream"].wait()
    resid[...] = f32(stream[...])
    loads["out"].wait()
    loads["norm"].wait()
    landed(weights_all.at[first], wq_recv_sems.at[first])
    send(
        weights_all.at[first],
        weights_all.at[first],
        w_send_sems.at[tp_count + 1],
        wq_recv_sems.at[first],
        to_second,
    )
    wide = heads * HD
    strip = 512 if width % 512 == 0 else width
    for at, level in enumerate(levels):
        for side in (core, other):
            source = level * 2 + side
            own = at == 0 and side is core
            part = leaving if own else incoming
            if not own:
                landed(incoming.at[source], out_recv_sems.at[source])

            @pl.loop(0, width // strip)
            def _(j, part=part, source=source):
                cols = pl.ds(pl.multiple_of(j * strip, strip), strip)
                weights = out_w[pl.ds(pl.multiple_of(source * wide, wide), wide), cols]
                resid[:, cols] += jnp.dot(
                    part[source], weights, preferred_element_type=jnp.float32
                )

    total = resid[...]
    center = total - jnp.mean(total, axis=1, keepdims=True)
    variance = jnp.mean(center * center, axis=1, keepdims=True)
    rows_all[core, z, sp] = (center * lax.rsqrt(variance + 1e-05) * norm_gain[0:1, :]).astype(
        jnp.bfloat16
    )

    ag_count = [0]

    def spread(level, quad, target, when=None):
        ref = rows_all.at[core, level, quad]
        sem = ag_recv_sems.at[core, level, quad]
        send(ref, ref, ag_send_sems.at[ag_count[0]], sem, target, when)
        ag_count[0] += 1

    def arrived(half, level, quad):
        landed(rows_all.at[half, level, quad], ag_recv_sems.at[half, level, quad])

    above, below = at_z((z + 1) % depth), at_z((z + depth - 1) % depth)
    spread(z, sp, above, z < depth - 1)
    spread(z, sp, below, z > 0)
    for target in (to_first, to_second, to_core):
        spread(z, sp, target)

    landed(weights_all.at[second], wq_recv_sems.at[second])
    landed(weights_all.at[far], wq_recv_sems.at[far])
    lane = lax.broadcasted_iota(jnp.int32, (QUADS, LANES), 0)
    picked = []
    for quad in range(QUADS):
        for source in range(tp_count):
            tile = weights_all[quad, source]
            picked.append(jnp.sum(jnp.where(lane == sp, tile, 0.0), axis=0, keepdims=True))
    fill = jnp.zeros((LANES - len(picked), LANES), jnp.float32)
    turned = jnp.transpose(jnp.concatenate(picked + [fill], axis=0))
    for quad in range(QUADS):
        for source in range(tp_count):
            at = quad * tp_count + source
            wcols[source % 2, source // 2, quad] = turned[:count, at : at + 1]

    for name in ("gate", "up", "down"):
        loads[name].wait()

    def experts(half, level, dest):
        piece = 256 if units % 256 == 0 else units

        @pl.loop(0, units // piece)
        def _(j):
            cols = pl.ds(pl.multiple_of(j * piece, piece), piece)
            block = rows_all[half, level].reshape(QUADS * count, width)
            gate_pre = jnp.dot(block, gate_w[:, cols], preferred_element_type=jnp.float32)
            up_pre = jnp.dot(block, up_w[:, cols], preferred_element_type=jnp.float32)
            hidden[:, cols] = (gate_pre / (1.0 + jnp.exp(-gate_pre)) * up_pre).astype(jnp.bfloat16)

        @pl.loop(0, width // strip)
        def _(j):
            cols = pl.ds(pl.multiple_of(j * strip, strip), strip)
            weight = wcols[half, level].reshape(QUADS * count, 1)
            product = jnp.dot(hidden[...], down_w[:, cols], preferred_element_type=jnp.float32)
            dest[level, :, :, cols] = bf16(product * weight).reshape(QUADS, count, strip)

    rs_count = [0]

    def send_back(src, dst, sem, target, when=None):
        send(src, dst, rs_send_sems.at[rs_count[0]], sem, target, when)
        rs_count[0] += 1

    def from_z_near(place):
        level = levels[place]
        arrived(core, level, sp)
        spread(level, sp, above, (level < z) & (z < depth - 1))
        spread(level, sp, below, (level > z) & (z > 0))
        spread(level, sp, to_first, (level - z) * (level - z) != 1)
        spread(level, sp, to_second)
        spread(level, sp, to_core)

    def from_first_near(place):
        level = levels[place]
        arrived(core, level, first)
        if place == 0:
            spread(level, first, above, z < depth - 1)
            spread(level, first, below, z > 0)
        spread(level, first, to_second)
        spread(level, first, to_core)

    def from_second_near(place):
        arrived(core, levels[place], second)
        spread(levels[place], second, to_core)

    def from_far(place):
        arrived(core, levels[place], far)
        spread(levels[place], far, to_core)

    def own_half(place):
        experts(core, levels[place], mine)

    def partner_half(place):
        level = levels[place]
        for quad in range(QUADS):
            arrived(other, level, quad)
        experts(other, level, theirs)
        send_back(theirs.at[level], from_core.at[level], core_sems.at[level], to_core)

    def both_halves(place):
        level = levels[place]
        landed(from_core.at[level], core_sems.at[level])
        for slot, quad in ((1, far), (0, second)):
            mine[level, quad] = bf16(f32(mine[level, quad]) + f32(from_core[level, quad]))
            send_back(
                mine.at[level, quad],
                from_second.at[level, slot],
                second_sems.at[level, slot],
                to_second,
            )

    def onto_first(place):
        level = levels[place]
        landed(from_second.at[level, 1], second_sems.at[level, 1])
        if place == 0:
            for near in levels[1:]:

                @pl.when(adjacent(near))
                def _(near=near):
                    landed(from_zf.at[near], zf_sems.at[near])
                    mine[z, first] = bf16(f32(mine[z, first]) + f32(from_zf[near]))

        mine[level, first] = bf16(
            f32(mine[level, first]) + f32(from_core[level, first]) + f32(from_second[level, 1])
        )
        src = mine.at[level, first]
        if place:
            near = adjacent(level)
            send_back(src, from_zf.at[z], zf_sems.at[z], at_z(level), near)
            apart = (level - z) * (level - z) != 1
            send_back(src, from_first.at[level], first_sems.at[level], to_first, apart)
        else:
            send_back(src, from_first.at[level], first_sems.at[level], to_first)

    def onto_owner(place):
        level = levels[place]
        landed(from_second.at[level, 0], second_sems.at[level, 0])
        if place:

            @pl.when((level - z) * (level - z) != 1)
            def _():
                landed(from_first.at[level], first_sems.at[level])
                mine[level, sp] = bf16(
                    f32(mine[level, sp])
                    + f32(from_core[level, sp])
                    + f32(from_second[level, 0])
                    + f32(from_first[level])
                )

            @pl.when(adjacent(level))
            def _():
                mine[level, sp] = bf16(
                    f32(mine[level, sp])
                    + f32(from_core[level, sp])
                    + f32(from_second[level, 0])
                )

            send_back(mine.at[level, sp], from_z.at[z], z_sems.at[z], at_z(level))
        else:
            landed(from_first.at[level], first_sems.at[level])
            resid[...] += (
                f32(mine[level, sp])
                + f32(from_core[level, sp])
                + f32(from_second[level, 0])
                + f32(from_first[level])
            )

    tasks = dict(
        zar=from_z_near,
        far=from_first_near,
        s=from_second_near,
        f=from_far,
        co=own_half,
        cp=partner_half,
        r1=both_halves,
        r2=onto_first,
        r3=onto_owner,
    )
    for name, place in TASKS:
        tasks[name](place)

    total = resid[...]
    for near in levels[1:]:
        landed(from_z.at[near], z_sems.at[near])
        total = total + f32(from_z[near])
    out_ref[...] = total.astype(out_ref.dtype)
    for copy, when in sent:
        if when is None:
            copy.wait_send()
        else:
            pl.when(when)(copy.wait_send)


def whole_layer(
    queries,
    keys,
    values,
    forget_totals,
    head_gain,
    stream,
    out_weight,
    norm_gain,
    routing,
    route_weights,
    gate_weight,
    up_weight,
    down_weight,
):
    tokens, wide = queries.shape
    heads = wide // HD
    count, width = stream.shape
    units = gate_weight.shape[2]
    tp_count = lax.axis_size("tp")
    depth = tp_count // 2
    top = routing.shape[1]
    bf16, f32 = jnp.bfloat16, jnp.float32
    dma = pltpu.SemaphoreType.DMA
    vmem = pltpu.VMEM
    plane = (depth, QUADS, count, width)
    hbm = pl.BlockSpec(memory_space=pltpu.HBM)
    ag_sends = 5 + 5 * (depth - 1) + 2 * depth + 2 + 2 * depth
    rs_sends = depth + 2 * depth + 2 * depth + depth
    return pl.pallas_call(
        partial(layer_kernel, depth),
        out_shape=jax.ShapeDtypeStruct((count, width), bf16),
        in_specs=[hbm] * 13,
        out_specs=pl.BlockSpec(memory_space=pltpu.VMEM),
        scratch_shapes=[
            vmem((tokens, wide), bf16),
            vmem((count, width), bf16),
            vmem((1, wide), f32),
            vmem((1, width), f32),
            vmem((top, count), jnp.int32),
            vmem((top, count), f32),
            vmem((QUADS, tokens, wide), bf16),
            vmem((QUADS, tokens, wide), bf16),
            vmem((QUADS, heads, tokens), f32),
            vmem((QUADS, tp_count, QUADS, LANES), f32),
            vmem((2, depth, QUADS, count, 1), f32),
            vmem((heads, tokens, 1), f32),
            vmem((heads, tokens, 1), f32),
            vmem((heads, tokens, 1), f32),
            vmem((heads, tokens, HD), f32),
            vmem((tp_count, count, wide), bf16),
            vmem((tp_count, count, wide), bf16),
            vmem((count, width), f32),
            vmem(out_weight.shape, bf16),
            vmem((2,) + plane, bf16),
            vmem((width, units), bf16),
            vmem((width, units), bf16),
            vmem((units, width), bf16),
            vmem((QUADS * count, units), bf16),
            vmem(plane, bf16),
            vmem(plane, bf16),
            vmem(plane, bf16),
            vmem((depth, 2, count, width), bf16),
            vmem((depth, count, width), bf16),
            vmem((depth, count, width), bf16),
            vmem((depth, count, width), bf16),
            dma((13,)),
            dma((9,)),
            dma((QUADS, 3)),
            dma((tp_count,)),
            dma((tp_count,)),
            dma((tp_count + 2,)),
            dma((tp_count,)),
            dma((QUADS,)),
            dma((ag_sends,)),
            dma((2, depth, QUADS)),
            dma((rs_sends,)),
            dma((depth,)),
            dma((depth, 2)),
            dma((depth,)),
            dma((depth,)),
            dma((depth,)),
        ],
        compiler_params=pltpu.CompilerParams(
            collective_id=0, has_side_effects=True, vmem_limit_bytes=58 * 2**20
        ),
    )(
        queries,
        keys,
        values,
        jnp.transpose(forget_totals),
        head_gain.reshape(1, -1),
        stream,
        out_weight,
        norm_gain.reshape(1, -1),
        jnp.transpose(routing),
        jnp.transpose(route_weights),
        gate_weight,
        up_weight,
        down_weight,
    )


def routed_experts(
    resid_sum, normed_rows, routing, route_weights, gate_weight, up_weight, down_weight
):
    sp_count = lax.axis_size("sp")
    row_count = normed_rows.shape[0]
    capacity = max(2, 2 * TOP * row_count // sp_count)
    flat_expert = routing.reshape(-1)
    onehot = (flat_expert[:, None] == jnp.arange(sp_count, dtype=jnp.int32)[None, :]).astype(
        jnp.int32
    )
    earlier = jnp.cumsum(onehot, axis=0) - onehot
    slot_index = flat_expert * capacity + jnp.sum(earlier * onehot, axis=1)
    slot_grid = slot_index.reshape(row_count, TOP)
    slot_ids = jnp.arange(sp_count * capacity, dtype=jnp.int32)
    placing = jnp.sum(
        (slot_grid[None, :, :] == slot_ids[:, None, None]).astype(jnp.float32), axis=2
    ).astype(jnp.bfloat16)
    outgoing = jnp.dot(placing, normed_rows, preferred_element_type=jnp.float32).astype(
        jnp.bfloat16
    )
    outgoing = outgoing.reshape(sp_count, capacity, normed_rows.shape[1])
    arrived = lax.all_to_all(outgoing, "sp", split_axis=0, concat_axis=0, tiled=True)
    row_piece = lax.all_gather(arrived.reshape(-1, arrived.shape[2]), "tp", axis=0, tiled=True)
    gate_pre = jnp.dot(row_piece, gate_weight[0], preferred_element_type=jnp.float32)
    up_pre = jnp.dot(row_piece, up_weight[0], preferred_element_type=jnp.float32)
    hidden = (jax.nn.silu(gate_pre) * up_pre).astype(jnp.bfloat16)
    summed = lax.psum_scatter(
        jnp.dot(hidden, down_weight[0], preferred_element_type=jnp.float32).astype(jnp.bfloat16),
        "tp",
        scatter_dimension=0,
        tiled=True,
    )
    expert_out = summed.reshape(sp_count, capacity, -1)
    returned = lax.all_to_all(expert_out, "sp", split_axis=0, concat_axis=0, tiled=True)
    picked = returned.reshape(sp_count * capacity, -1)[slot_index].astype(jnp.float32)
    weighted = picked * route_weights.reshape(-1)[:, None]
    routed = jnp.sum(weighted.reshape(row_count, TOP, -1), axis=1)
    return (resid_sum + routed).astype(jnp.bfloat16)


def on_device(
    queries,
    key_vectors,
    value_vectors,
    forget_totals,
    head_gain,
    stream,
    out_weight,
    norm_gain,
    routing,
    route_weights,
    gate_weight,
    up_weight,
    down_weight,
):
    rows_dev, sp_size, tp_size = stream.shape[0], lax.axis_size("sp"), lax.axis_size("tp")
    dense = 2 * TOP * rows_dev // sp_size >= rows_dev
    leveled = sp_size == QUADS and tp_size == 2 * len({place for _, place in TASKS})
    if dense and leveled and queries.shape[0] % LANES == 0 and rows_dev <= LANES:
        return whole_layer(
            queries,
            key_vectors,
            value_vectors,
            forget_totals,
            head_gain,
            stream,
            out_weight,
            norm_gain,
            routing,
            route_weights,
            gate_weight,
            up_weight,
            down_weight,
        )
    tok_count = queries.shape[0]
    heads_dev = queries.shape[1] // HD
    sp_index = lax.axis_index("sp")
    sp_count = lax.axis_size("sp")
    gathered_gates = lax.all_gather(forget_totals, "sp", axis=0, tiled=True)
    first_pos = sp_index * tok_count
    query_pos = first_pos + jnp.arange(tok_count, dtype=jnp.int32)
    query_gate = jnp.transpose(lax.dynamic_slice_in_dim(gathered_gates, first_pos, tok_count, 0))
    segments = [(queries.reshape(tok_count, heads_dev, HD), query_gate, query_pos)]
    starting = (
        (
            jnp.full((heads_dev, tok_count), masked_score, jnp.float32),
            jnp.zeros((heads_dev, tok_count), jnp.float32),
            jnp.zeros((heads_dev, tok_count, HD), jnp.float32),
        ),
    )
    folder = make_folder(segments, gathered_gates)
    totals = folder(
        starting,
        (
            lax.all_gather(key_vectors, "sp", axis=0, tiled=True),
            lax.all_gather(value_vectors, "sp", axis=0, tiled=True),
        ),
        jnp.int32(0),
    )
    run_max, run_sum, run_acc = totals[0]
    attended = run_acc / run_sum[:, :, None]
    inverse_rms = lax.rsqrt(jnp.mean(attended * attended, axis=2, keepdims=True) + 1e-06)
    normed = attended * inverse_rms * head_gain.reshape(heads_dev, 1, HD)
    head_out = (
        jnp.transpose(normed, (1, 0, 2)).reshape(tok_count, heads_dev * HD).astype(jnp.bfloat16)
    )
    token_heads = lax.all_to_all(head_out, "tp", split_axis=0, concat_axis=1, tiled=True)
    mixed_rows = jnp.dot(token_heads, out_weight, preferred_element_type=jnp.float32)
    resid_sum = stream.astype(jnp.float32) + mixed_rows
    center = resid_sum - jnp.mean(resid_sum, axis=1, keepdims=True)
    normed_rows = (
        center * lax.rsqrt(jnp.mean(center * center, axis=1, keepdims=True) + 1e-05) * norm_gain
    ).astype(jnp.bfloat16)
    return routed_experts(
        resid_sum, normed_rows, routing, route_weights, gate_weight, up_weight, down_weight
    )


def solution(mesh):
    in_specs = (
        P("sp", "tp"),
        P("sp", "tp"),
        P("sp", "tp"),
        P("sp", "tp"),
        P("tp"),
        P(("sp", "tp"), None),
        P(),
        P(),
        P(("sp", "tp"), None),
        P(("sp", "tp"), None),
        P("sp", None, "tp"),
        P("sp", None, "tp"),
        P("sp", "tp", None),
    )
    out_specs = P(("sp", "tp"), None)
    return jax.shard_map(
        on_device, mesh=mesh, in_specs=in_specs, out_specs=out_specs, check_vma=False
    )
```

time: 164 us -> 122 us (0.74)
  Pallas kernels: 152 us -> 120 us
  local copies, waits for them, and re-layouts: 10.9 us -> 1.67 us
    pallas_call x2 -> x1, Pallas kernels: 152 us -> 120 us  [whole_layer(): pl.pallas_call(partial(layer_kernel, depth), out_shape=jax.ShapeDtypeStru...]
    unnamed x20 -> x1, local copies, waits for them, and re-layouts: 10.1 us -> 1.67 us
where the time goes in v1:
time: 122 us
  Pallas kernels  120 us (98%)
  local copies, waits for them, and re-layouts  1.67 us (1%)
    pallas_call x1, Pallas kernels, whole_layer(): pl.pallas_call(partial(layer_kernel, depth), out_shape=jax.ShapeDtypeStru...  120 us

profile of v1, /device:TPU:0, one launch (start us, length us, event | category | flops | bytes accessed | tf_op | source)
XLA Modules:
  0.0 122.0 jit_solution(9530180981480949719)
XLA Ops:
  0.0 120.3 %shard_map.127 = bf16[64,2048]{1,0:T(8,128)(2,1)} custom-call(bf16[512,256]{1,0:T(8,128)(2,1)} %queries_hbm.1, bf16[512,256]{1,0:T(8,128)(2,1)} %keys_hbm.1, bf16[512,256]{1,0:T(8,128)(2,1)} %values_hbm.1, f32[2,512]{1,0:T(2,128)} %bitcast.6, f32[1,256]{1,0:T(1,128)} %bitcast.7, bf16[64,2048]{1,0:T(8,128)(2,1)} %stream_hbm.1, bf16[2048,2048]{1,0:T(8,128)(2,1)} %out_hbm.1, ...), custom_call_target="tpu_custom_call" | custom-call | tf_op jit(solution)/shard_map/pallas_call | solution.py:670
  120.3 1.7 %copy.15 = bf16[64,2048]{1,0:T(8,128)(2,1)} copy(bf16[64,2048]{1,0:T(8,128)(2,1)} %shard_map.127) | data formatting | bytes 524288

commit v2 on v1

--- a/solution.py
+++ b/solution.py
@@ -79,40 +79,49 @@
 LANES = 128
 QUADS = 4
 LOG2E = 1.4426950408889634
+PARTS = 2
 
 TASKS = (
-    ("far", 0),
-    ("zar", 1),
-    ("zar", 2),
+    ("zr", 1),
+    ("fa", 0),
+    ("zr", 2),
+    ("fa", 1),
+    ("s", 1),
+    ("fa", 2),
+    ("d", 0),
     ("s", 0),
-    ("f", 0),
-    ("far", 1),
-    ("co", 0),
-    ("zar", 3),
-    ("cp", 0),
-    ("far", 2),
-    ("s", 1),
-    ("f", 1),
-    ("co", 1),
-    ("far", 3),
+    ("co1", 0),
+    ("zr", 3),
+    ("d", 1),
+    ("s", 2),
+    ("co1", 1),
+    ("cp1", 1),
+    ("d", 2),
+    ("cp2", 1),
+    ("fa", 3),
+    ("co1", 2),
+    ("co2", 1),
+    ("r1", 1),
+    ("cp1", 2),
+    ("d", 3),
+    ("cp2", 2),
+    ("s", 3),
+    ("r2", 1),
+    ("co2", 2),
+    ("r1", 2),
+    ("cp1", 3),
+    ("r3", 1),
+    ("co1", 3),
+    ("cp2", 3),
+    ("r2", 2),
+    ("co2", 0),
+    ("co2", 3),
+    ("r1", 3),
+    ("r3", 2),
+    ("cp1", 0),
+    ("cp2", 0),
+    ("r2", 3),
     ("r1", 0),
-    ("cp", 1),
-    ("s", 2),
-    ("f", 2),
-    ("co", 2),
-    ("r1", 1),
-    ("cp", 2),
-    ("r1", 2),
-    ("s", 3),
-    ("f", 3),
-    ("co", 3),
-    ("cp", 3),
-    ("r2", 1),
-    ("r3", 1),
-    ("r1", 3),
-    ("r2", 2),
-    ("r3", 2),
-    ("r2", 3),
     ("r3", 3),
     ("r2", 0),
     ("r3", 0),
@@ -190,6 +199,7 @@
     heads = queries.shape[1] // HD
     count, width = resid.shape
     units = gate_w.shape[1]
+    part_rows = count // PARTS
     z, core = tp // 2, tp % 2
     other = 1 - core
     x_next = sp + 1 - 2 * (sp % 2)
@@ -214,7 +224,8 @@
     for at in range(depth):
         order = [at]
         for step in range(1, depth):
-            order += [lev for lev in (at - step, at + step) if 0 <= lev < depth]
+            pair = (at + step, at - step) if 2 * at < depth else (at - step, at + step)
+            order += [lev for lev in pair if 0 <= lev < depth]
         orders.append(order)
     levels = []
     for place in range(depth):
@@ -233,9 +244,13 @@
         loads[name] = pltpu.make_async_copy(src, dst, local_sems.at[len(loads)])
         loads[name].start()
 
-    load("keys", keys_hbm, key_all.at[sp])
-    load("values", values_hbm, value_all.at[sp])
+    def head_cols(head):
+        return slice(head * HD, (head + 1) * HD)
+
     load("gates", gates_hbm, gate_all.at[sp])
+    for head in range(heads):
+        load(("keys", head), keys_hbm.at[:, head_cols(head)], key_all.at[sp, head])
+        load(("values", head), values_hbm.at[:, head_cols(head)], value_all.at[sp, head])
     load("queries", queries_hbm, queries)
     load("routing", routing_hbm, routing)
     load("route", route_hbm, route_w)
@@ -274,25 +289,33 @@
             device_id_type=MESH,
         ).wait_recv()
 
-    kv_refs = (key_all, value_all, gate_all)
+    def kv_refs(quad, head):
+        refs = [(key_all.at[quad, head], 2 * head), (value_all.at[quad, head], 2 * head + 1)]
+        return refs if head else [(gate_all.at[quad], 2 * heads)] + refs
+
     kv_count = [0]
 
-    def kv_send(quad, part, target):
-        ref = kv_refs[part].at[quad]
-        send(ref, ref, kv_send_sems.at[kv_count[0]], kv_recv_sems.at[quad, part], target)
-        kv_count[0] += 1
-
-    def kv_landed(quad, part):
-        landed(kv_refs[part].at[quad], kv_recv_sems.at[quad, part])
-
-    for part, name in enumerate(("keys", "values", "gates")):
-        loads[name].wait()
-        kv_send(sp, part, to_first)
-        kv_send(sp, part, to_second)
+    def kv_send(quad, head, target):
+        for ref, part in kv_refs(quad, head):
+            send(ref, ref, kv_send_sems.at[kv_count[0]], kv_recv_sems.at[quad, part], target)
+            kv_count[0] += 1
+
+    def kv_landed(quad, head):
+        for ref, part in kv_refs(quad, head):
+            landed(ref, kv_recv_sems.at[quad, part])
+
+    loads["gates"].wait()
+    for head in range(heads):
+        loads["keys", head].wait()
+        loads["values", head].wait()
+        kv_send(sp, head, to_first)
+        if head == 0:
+            kv_send(sp, head, to_second)
     load("stream", stream_hbm, stream)
     load("gain", gain_hbm, gain)
     load("norm", norm_hbm, norm_gain)
-    load("out", out_hbm, out_w)
+    for head in range(heads):
+        load(("out", head), out_hbm.at[:, head], out_w.at[head])
     load("gate", gate_hbm.at[0], gate_w)
     load("up", up_hbm.at[0], up_w)
     load("down", down_hbm.at[0], down_w)
@@ -316,93 +339,114 @@
             row = gate_all[sp, head : head + 1, span] * LOG2E
             qcol[head, span] = jnp.transpose(jnp.broadcast_to(row, (chunk, chunk)))[:, :1]
 
-    def attend(quad, diagonal):
-        @pl.loop(0, tokens // chunk)
+    def attend(quad, head, diagonal):
+        cols = head_cols(head)
+
+        def attend_chunk(j):
+            rows = pl.ds(pl.multiple_of(j * chunk, chunk), chunk)
+            scores = lax.dot_general(
+                queries[rows, cols],
+                key_all[quad, head],
+                (((1,), (1,)), ((), ())),
+                preferred_element_type=jnp.float32,
+            )
+            query_gate = qcol[head, rows]
+            key_gate = gate_all[quad, head : head + 1, :] * LOG2E
+            scores = scores * (HD ** (-0.5) * LOG2E) - key_gate
+            if diagonal:
+                row_id = lax.broadcasted_iota(jnp.int32, scores.shape, 0) + j * chunk
+                col_id = lax.broadcasted_iota(jnp.int32, scores.shape, 1)
+                scores = jnp.where(col_id <= row_id, scores, masked_score)
+            new_peak = jnp.max(scores, axis=1, keepdims=True) + query_gate
+            if not diagonal:
+                old_peak = peak[head, rows]
+                new_peak = jnp.maximum(old_peak, new_peak)
+            lifted = jnp.exp2(scores + (query_gate - new_peak))
+            added = jnp.sum(lifted, axis=1, keepdims=True)
+            product = jnp.dot(
+                lifted.astype(jnp.bfloat16),
+                value_all[quad, head],
+                preferred_element_type=jnp.float32,
+            )
+            if not diagonal:
+                rescale = jnp.exp2(old_peak - new_peak)
+                added = weight_total[head, rows] * rescale + added
+                product = weighted[head, rows] * rescale + product
+            peak[head, rows] = new_peak
+            weight_total[head, rows] = added
+            weighted[head, rows] = product
+
+        pairs = 2 if tokens % (2 * chunk) == 0 else 1
+
+        @pl.loop(0, tokens // (pairs * chunk))
         def _(j):
-            rows = pl.ds(pl.multiple_of(j * chunk, chunk), chunk)
-            for head in range(heads):
-                cols = slice(head * HD, (head + 1) * HD)
-                scores = lax.dot_general(
-                    queries[rows, cols],
-                    key_all[quad, :, cols],
-                    (((1,), (1,)), ((), ())),
-                    preferred_element_type=jnp.float32,
-                )
-                query_gate = qcol[head, rows]
-                key_gate = gate_all[quad, head : head + 1, :] * LOG2E
-                scores = scores * (HD ** (-0.5) * LOG2E) - key_gate
-                if diagonal:
-                    row_id = lax.broadcasted_iota(jnp.int32, scores.shape, 0) + j * chunk
-                    col_id = lax.broadcasted_iota(jnp.int32, scores.shape, 1)
-                    scores = jnp.where(col_id <= row_id, scores, masked_score)
-                new_peak = jnp.max(scores, axis=1, keepdims=True) + query_gate
-                if not diagonal:
-                    old_peak = peak[head, rows]
-                    new_peak = jnp.maximum(old_peak, new_peak)
-                lifted = jnp.exp2(scores + (query_gate - new_peak))
-                added = jnp.sum(lifted, axis=1, keepdims=True)
-                product = jnp.dot(
-                    lifted.astype(jnp.bfloat16),
-                    value_all[quad, :, cols],
-                    preferred_element_type=jnp.float32,
-                )
-                if not diagonal:
-                    rescale = jnp.exp2(old_peak - new_peak)
-                    added = weight_total[head, rows] * rescale + added
-                    product = weighted[head, rows] * rescale + product
-                peak[head, rows] = new_peak
-                weight_total[head, rows] = added
-                weighted[head, rows] = product
-
-    def attend_earlier(quad):
+            for at in range(pairs):
+                attend_chunk(j * pairs + at)
+
+    def attend_earlier(quad, head):
         @pl.when(quad < sp)
         def _():
-            attend(quad, False)
-
-    attend(sp, True)
+            attend(quad, head, False)
+
+    def take_first(head):
+        kv_landed(first, head)
+        kv_send(first, head, to_second)
+        if head + 1 < heads:
+            kv_send(sp, head + 1, to_second)
+        attend_earlier(first, head)
+
+    def take_second(head):
+        kv_landed(second, head)
+        attend_earlier(second, head)
+
+    out_count = [0]
+
+    def finish(head):
+        kv_landed(far, head)
+        attend_earlier(far, head)
+
+        @pl.loop(0, tp_count)
+        def _(j):
+            rows = pl.ds(pl.multiple_of(j * count, count), count)
+            attended = weighted[head, rows] / weight_total[head, rows]
+            square = jnp.mean(attended * attended, axis=1, keepdims=True)
+            normed = attended * lax.rsqrt(square + 1e-06) * gain[0:1, head_cols(head)]
+            leaving[head, j] = normed.astype(jnp.bfloat16)
+
+        for level in reversed(levels):
+            for side in (core, other):
+                if level is z_level and side is core:
+                    continue
+                target = level * 2 + side
+                send(
+                    leaving.at[head, target],
+                    incoming.at[head, tp],
+                    out_send_sems.at[out_count[0]],
+                    out_recv_sems.at[head, tp],
+                    (sp, target),
+                )
+                out_count[0] += 1
+        incoming[head, tp] = leaving[head, tp]
+
+    z_level = levels[0]
+    for head in range(heads):
+        attend(sp, head, True)
     for step in range(1, tp_count):
         target = (tp + step) % tp_count
         ref = weights_all.at[sp, tp]
         send(ref, ref, w_send_sems.at[step], w_recv_sems.at[tp], (sp, target))
-    for part in range(3):
-        kv_landed(first, part)
-        kv_send(first, part, to_second)
-    attend_earlier(first)
-    for part in range(3):
-        kv_landed(second, part)
-    attend_earlier(second)
+    loads["gain"].wait()
+    take_first(0)
+    take_second(0)
+    for head in range(heads):
+        if head + 1 < heads:
+            take_first(head + 1)
+        finish(head)
+        if head + 1 < heads:
+            take_second(head + 1)
     for step in range(1, tp_count):
         source = (tp + step) % tp_count
         landed(weights_all.at[sp, source], w_recv_sems.at[source])
-    for part in range(3):
-        kv_landed(far, part)
-    attend_earlier(far)
-
-    loads["gain"].wait()
-
-    @pl.loop(0, tp_count)
-    def _(j):
-        rows = pl.ds(pl.multiple_of(j * count, count), count)
-        for head in range(heads):
-            cols = slice(head * HD, (head + 1) * HD)
-            attended = weighted[head, rows] / weight_total[head, rows]
-            square = jnp.mean(attended * attended, axis=1, keepdims=True)
-            normed = attended * lax.rsqrt(square + 1e-06) * gain[0:1, cols]
-            leaving[j, :, cols] = normed.astype(jnp.bfloat16)
-
-    for at, level in enumerate(reversed(levels)):
-        for side in (core, other):
-            if at == depth - 1 and side is core:
-                continue
-            target = level * 2 + side
-            index = 2 * at + (0 if side is core else 1)
-            send(
-                leaving.at[target],
-                incoming.at[tp],
-                out_send_sems.at[index],
-                out_recv_sems.at[tp],
-                (sp, target),
-            )
 
     send(weights_all.at[sp], weights_all.at[sp], w_send_sems.at[0], wq_recv_sems.at[sp], to_first)
     send(
@@ -414,7 +458,6 @@
     )
     loads["stream"].wait()
     resid[...] = f32(stream[...])
-    loads["out"].wait()
     loads["norm"].wait()
     landed(weights_all.at[first], wq_recv_sems.at[first])
     send(
@@ -424,23 +467,22 @@
         wq_recv_sems.at[first],
         to_second,
     )
-    wide = heads * HD
     strip = 512 if width % 512 == 0 else width
-    for at, level in enumerate(levels):
-        for side in (core, other):
-            source = level * 2 + side
-            own = at == 0 and side is core
-            part = leaving if own else incoming
-            if not own:
-                landed(incoming.at[source], out_recv_sems.at[source])
+    for head in range(heads):
+        loads["out", head].wait()
+        for level in levels:
+            sources = (level * 2, level * 2 + 1)
+            for side in (core, other):
+                source = level * 2 + side
+                if not (level is z_level and side is core):
+                    landed(incoming.at[head, source], out_recv_sems.at[head, source])
 
             @pl.loop(0, width // strip)
-            def _(j, part=part, source=source):
+            def _(j, head=head, level=level, sources=sources):
                 cols = pl.ds(pl.multiple_of(j * strip, strip), strip)
-                weights = out_w[pl.ds(pl.multiple_of(source * wide, wide), wide), cols]
-                resid[:, cols] += jnp.dot(
-                    part[source], weights, preferred_element_type=jnp.float32
-                )
+                rows = jnp.concatenate([incoming[head, source] for source in sources], axis=1)
+                weights = out_w[head, pl.ds(level * 2, 2), :, cols].reshape(2 * HD, strip)
+                resid[:, cols] += jnp.dot(rows, weights, preferred_element_type=jnp.float32)
 
     total = resid[...]
     center = total - jnp.mean(total, axis=1, keepdims=True)
@@ -451,20 +493,25 @@
 
     ag_count = [0]
 
-    def spread(level, quad, target, when=None):
-        ref = rows_all.at[core, level, quad]
-        sem = ag_recv_sems.at[core, level, quad]
+    def part_of(k):
+        return pl.ds(k * part_rows, part_rows)
+
+    def spread(level, quad, k, target, when=None):
+        ref = rows_all.at[core, level, quad, part_of(k)]
+        sem = ag_recv_sems.at[core, level, quad, k]
         send(ref, ref, ag_send_sems.at[ag_count[0]], sem, target, when)
         ag_count[0] += 1
 
-    def arrived(half, level, quad):
-        landed(rows_all.at[half, level, quad], ag_recv_sems.at[half, level, quad])
+    def arrived(half, level, quad, k):
+        ref = rows_all.at[half, level, quad, part_of(k)]
+        landed(ref, ag_recv_sems.at[half, level, quad, k])
 
     above, below = at_z((z + 1) % depth), at_z((z + depth - 1) % depth)
-    spread(z, sp, above, z < depth - 1)
-    spread(z, sp, below, z > 0)
-    for target in (to_first, to_second, to_core):
-        spread(z, sp, target)
+    for k in range(PARTS):
+        spread(z, sp, k, above, z < depth - 1)
+        spread(z, sp, k, below, z > 0)
+        for target in (to_first, to_second, to_core):
+            spread(z, sp, k, target)
 
     landed(weights_all.at[second], wq_recv_sems.at[second])
     landed(weights_all.at[far], wq_recv_sems.at[far])
@@ -484,8 +531,8 @@
     for name in ("gate", "up", "down"):
         loads[name].wait()
 
-    def experts(half, level, dest):
-        piece = 256 if units % 256 == 0 else units
+    def hidden_units(half, level):
+        piece = 512 if units % 512 == 0 else units
 
         @pl.loop(0, units // piece)
         def _(j):
@@ -493,14 +540,17 @@
             block = rows_all[half, level].reshape(QUADS * count, width)
             gate_pre = jnp.dot(block, gate_w[:, cols], preferred_element_type=jnp.float32)
             up_pre = jnp.dot(block, up_w[:, cols], preferred_element_type=jnp.float32)
-            hidden[:, cols] = (gate_pre / (1.0 + jnp.exp(-gate_pre)) * up_pre).astype(jnp.bfloat16)
-
-        @pl.loop(0, width // strip)
+            hidden[half, level, :, cols] = bf16(gate_pre / (1.0 + jnp.exp(-gate_pre)) * up_pre)
+
+    def down_product(half, level, dest):
+        piece = 1024 if width % 1024 == 0 else width
+
+        @pl.loop(0, width // piece)
         def _(j):
-            cols = pl.ds(pl.multiple_of(j * strip, strip), strip)
+            cols = pl.ds(pl.multiple_of(j * piece, piece), piece)
             weight = wcols[half, level].reshape(QUADS * count, 1)
-            product = jnp.dot(hidden[...], down_w[:, cols], preferred_element_type=jnp.float32)
-            dest[level, :, :, cols] = bf16(product * weight).reshape(QUADS, count, strip)
+            product = jnp.dot(hidden[half, level], down_w[:, cols], preferred_element_type=jnp.float32)
+            dest[level, :, :, cols] = bf16(product * weight).reshape(QUADS, count, piece)
 
     rs_count = [0]
 
@@ -510,115 +560,134 @@
 
     def from_z_near(place):
         level = levels[place]
-        arrived(core, level, sp)
-        spread(level, sp, above, (level < z) & (z < depth - 1))
-        spread(level, sp, below, (level > z) & (z > 0))
-        spread(level, sp, to_first, (level - z) * (level - z) != 1)
-        spread(level, sp, to_second)
-        spread(level, sp, to_core)
+        for k in range(PARTS):
+            arrived(core, level, sp, k)
+            spread(level, sp, k, above, (level < z) & (z < depth - 1))
+            spread(level, sp, k, below, (level > z) & (z > 0))
+            spread(level, sp, k, to_first, (level - z) * (level - z) != 1)
+            spread(level, sp, k, to_second)
+            spread(level, sp, k, to_core)
 
     def from_first_near(place):
         level = levels[place]
-        arrived(core, level, first)
-        if place == 0:
-            spread(level, first, above, z < depth - 1)
-            spread(level, first, below, z > 0)
-        spread(level, first, to_second)
-        spread(level, first, to_core)
+        for k in range(PARTS):
+            arrived(core, level, first, k)
+            if place == 0:
+                spread(level, first, k, above, z < depth - 1)
+                spread(level, first, k, below, z > 0)
+            spread(level, first, k, to_second)
+            spread(level, first, k, to_core)
 
     def from_second_near(place):
-        arrived(core, levels[place], second)
-        spread(levels[place], second, to_core)
+        for k in range(PARTS):
+            arrived(core, levels[place], second, k)
+            spread(levels[place], second, k, to_core)
 
     def from_far(place):
-        arrived(core, levels[place], far)
-        spread(levels[place], far, to_core)
-
-    def own_half(place):
-        experts(core, levels[place], mine)
-
-    def partner_half(place):
+        for k in range(PARTS):
+            arrived(core, levels[place], far, k)
+            spread(levels[place], far, k, to_core)
+
+    def own_hidden(place):
+        hidden_units(core, levels[place])
+
+    def own_product(place):
+        down_product(core, levels[place], mine)
+
+    def partner_hidden(place):
         level = levels[place]
         for quad in range(QUADS):
-            arrived(other, level, quad)
-        experts(other, level, theirs)
+            for k in range(PARTS):
+                arrived(other, level, quad, k)
+        hidden_units(other, level)
+
+    def partner_product(place):
+        level = levels[place]
+        down_product(other, level, theirs)
         send_back(theirs.at[level], from_core.at[level], core_sems.at[level], to_core)
 
     def both_halves(place):
         level = levels[place]
         landed(from_core.at[level], core_sems.at[level])
         for slot, quad in ((1, far), (0, second)):
-            mine[level, quad] = bf16(f32(mine[level, quad]) + f32(from_core[level, quad]))
-            send_back(
-                mine.at[level, quad],
-                from_second.at[level, slot],
-                second_sems.at[level, slot],
-                to_second,
-            )
+            for k in range(PARTS):
+                rows = part_of(k)
+                mine[level, quad, rows] = bf16(
+                    f32(mine[level, quad, rows]) + f32(from_core[level, quad, rows])
+                )
+                send_back(
+                    mine.at[level, quad, rows],
+                    from_second.at[level, slot, rows],
+                    second_sems.at[level, slot, k],
+                    to_second,
+                )
 
     def onto_first(place):
         level = levels[place]
-        landed(from_second.at[level, 1], second_sems.at[level, 1])
         if place == 0:
             for near in levels[1:]:
 
                 @pl.when(adjacent(near))
                 def _(near=near):
-                    landed(from_zf.at[near], zf_sems.at[near])
+                    for k in range(PARTS):
+                        rows = part_of(k)
+                        landed(from_zf.at[near, rows], zf_sems.at[near, k])
                     mine[z, first] = bf16(f32(mine[z, first]) + f32(from_zf[near]))
 
-        mine[level, first] = bf16(
-            f32(mine[level, first]) + f32(from_core[level, first]) + f32(from_second[level, 1])
-        )
-        src = mine.at[level, first]
-        if place:
-            near = adjacent(level)
-            send_back(src, from_zf.at[z], zf_sems.at[z], at_z(level), near)
-            apart = (level - z) * (level - z) != 1
-            send_back(src, from_first.at[level], first_sems.at[level], to_first, apart)
-        else:
-            send_back(src, from_first.at[level], first_sems.at[level], to_first)
+        for k in range(PARTS):
+            rows = part_of(k)
+            landed(from_second.at[level, 1, rows], second_sems.at[level, 1, k])
+            mine[level, first, rows] = bf16(
+                f32(mine[level, first, rows])
+                + f32(from_core[level, first, rows])
+                + f32(from_second[level, 1, rows])
+            )
+            src = mine.at[level, first, rows]
+            dst, sem = from_first.at[level, rows], first_sems.at[level, k]
+            if place:
+                near = adjacent(level)
+                send_back(src, from_zf.at[z, rows], zf_sems.at[z, k], at_z(level), near)
+                send_back(src, dst, sem, to_first, (level - z) * (level - z) != 1)
+            else:
+                send_back(src, dst, sem, to_first)
 
     def onto_owner(place):
         level = levels[place]
-        landed(from_second.at[level, 0], second_sems.at[level, 0])
-        if place:
+        for k in range(PARTS):
+            rows = part_of(k)
+            landed(from_second.at[level, 0, rows], second_sems.at[level, 0, k])
+
+            def total_of(with_first, rows=rows):
+                total = f32(mine[level, sp, rows]) + f32(from_core[level, sp, rows])
+                total = total + f32(from_second[level, 0, rows])
+                return total + f32(from_first[level, rows]) if with_first else total
+
+            if place == 0:
+                landed(from_first.at[level, rows], first_sems.at[level, k])
+                resid[rows] += total_of(True)
+                continue
 
             @pl.when((level - z) * (level - z) != 1)
-            def _():
-                landed(from_first.at[level], first_sems.at[level])
-                mine[level, sp] = bf16(
-                    f32(mine[level, sp])
-                    + f32(from_core[level, sp])
-                    + f32(from_second[level, 0])
-                    + f32(from_first[level])
-                )
+            def _(k=k, rows=rows, total_of=total_of):
+                landed(from_first.at[level, rows], first_sems.at[level, k])
+                mine[level, sp, rows] = bf16(total_of(True))
 
             @pl.when(adjacent(level))
-            def _():
-                mine[level, sp] = bf16(
-                    f32(mine[level, sp])
-                    + f32(from_core[level, sp])
-                    + f32(from_second[level, 0])
-                )
-
-            send_back(mine.at[level, sp], from_z.at[z], z_sems.at[z], at_z(level))
-        else:
-            landed(from_first.at[level], first_sems.at[level])
-            resid[...] += (
-                f32(mine[level, sp])
-                + f32(from_core[level, sp])
-                + f32(from_second[level, 0])
-                + f32(from_first[level])
-            )
+            def _(rows=rows, total_of=total_of):
+                mine[level, sp, rows] = bf16(total_of(False))
+
+            src = mine.at[level, sp, rows]
+            send_back(src, from_z.at[z, rows], z_sems.at[z, k], at_z(level))
 
     tasks = dict(
-        zar=from_z_near,
-        far=from_first_near,
+        zr=from_z_near,
+        fa=from_first_near,
         s=from_second_near,
-        f=from_far,
-        co=own_half,
-        cp=partner_half,
+        d=from_far,
+        co1=own_hidden,
+        co2=own_product,
+        cp1=partner_hidden,
+        cp2=partner_product,
         r1=both_halves,
         r2=onto_first,
         r3=onto_owner,
@@ -628,7 +697,8 @@
 
     total = resid[...]
     for near in levels[1:]:
-        landed(from_z.at[near], z_sems.at[near])
+        for k in range(PARTS):
+            landed(from_z.at[near, part_of(k)], z_sems.at[near, k])
         total = total + f32(from_z[near])
     out_ref[...] = total.astype(out_ref.dtype)
     for copy, when in sent:
@@ -665,8 +735,8 @@
     vmem = pltpu.VMEM
     plane = (depth, QUADS, count, width)
     hbm = pl.BlockSpec(memory_space=pltpu.HBM)
-    ag_sends = 5 + 5 * (depth - 1) + 2 * depth + 2 + 2 * depth
-    rs_sends = depth + 2 * depth + 2 * depth + depth
+    ag_sends = PARTS * (5 + 5 * (depth - 1) + 2 * depth + 2 + 2 * depth)
+    rs_sends = depth + PARTS * (2 * depth + 2 * depth + depth)
     return pl.pallas_call(
         partial(layer_kernel, depth),
         out_shape=jax.ShapeDtypeStruct((count, width), bf16),
@@ -679,8 +749,8 @@
             vmem((1, width), f32),
             vmem((top, count), jnp.int32),
             vmem((top, count), f32),
-            vmem((QUADS, tokens, wide), bf16),
-            vmem((QUADS, tokens, wide), bf16),
+            vmem((QUADS, heads, tokens, HD), bf16),
+            vmem((QUADS, heads, tokens, HD), bf16),
             vmem((QUADS, heads, tokens), f32),
             vmem((QUADS, tp_count, QUADS, LANES), f32),
             vmem((2, depth, QUADS, count, 1), f32),
@@ -688,15 +758,15 @@
             vmem((heads, tokens, 1), f32),
             vmem((heads, tokens, 1), f32),
             vmem((heads, tokens, HD), f32),
-            vmem((tp_count, count, wide), bf16),
-            vmem((tp_count, count, wide), bf16),
+            vmem((heads, tp_count, count, HD), bf16),
+            vmem((heads, tp_count, count, HD), bf16),
             vmem((count, width), f32),
-            vmem(out_weight.shape, bf16),
+            vmem((heads, tp_count, HD, width), bf16),
             vmem((2,) + plane, bf16),
             vmem((width, units), bf16),
             vmem((width, units), bf16),
             vmem((units, width), bf16),
-            vmem((QUADS * count, units), bf16),
+            vmem((2, depth, QUADS * count, units), bf16),
             vmem(plane, bf16),
             vmem(plane, bf16),
             vmem(plane, bf16),
@@ -704,22 +774,22 @@
             vmem((depth, count, width), bf16),
             vmem((depth, count, width), bf16),
             vmem((depth, count, width), bf16),
-            dma((13,)),
-            dma((9,)),
-            dma((QUADS, 3)),
-            dma((tp_count,)),
-            dma((tp_count,)),
+            dma((10 + 3 * heads,)),
+            dma((3 + 6 * heads,)),
+            dma((QUADS, 1 + 2 * heads)),
+            dma((heads * (tp_count - 1),)),
+            dma((heads, tp_count)),
             dma((tp_count + 2,)),
             dma((tp_count,)),
             dma((QUADS,)),
             dma((ag_sends,)),
-            dma((2, depth, QUADS)),
+            dma((2, depth, QUADS, PARTS)),
             dma((rs_sends,)),
             dma((depth,)),
-            dma((depth, 2)),
-            dma((depth,)),
-            dma((depth,)),
-            dma((depth,)),
+            dma((depth, 2, PARTS)),
+            dma((depth, PARTS)),
+            dma((depth, PARTS)),
+            dma((depth, PARTS)),
         ],
         compiler_params=pltpu.CompilerParams(
             collective_id=0, has_side_effects=True, vmem_limit_bytes=58 * 2**20
@@ -731,7 +801,7 @@
         jnp.transpose(forget_totals),
         head_gain.reshape(1, -1),
         stream,
-        out_weight,
+        out_weight.reshape(tp_count, heads, HD, width),
         norm_gain.reshape(1, -1),
         jnp.transpose(routing),
         jnp.transpose(route_weights),
@@ -799,7 +869,7 @@
     rows_dev, sp_size, tp_size = stream.shape[0], lax.axis_size("sp"), lax.axis_size("tp")
     dense = 2 * TOP * rows_dev // sp_size >= rows_dev
     leveled = sp_size == QUADS and tp_size == 2 * len({place for _, place in TASKS})
-    if dense and leveled and queries.shape[0] % LANES == 0 and rows_dev <= LANES:
+    if dense and leveled and queries.shape[0] % LANES == 0 and rows_dev <= LANES and rows_dev % (16 * PARTS) == 0:
         return whole_layer(
             queries,
             key_vectors,

time: 122 us -> 108 us (0.89)
  Pallas kernels: 120 us -> 106 us
    pallas_call x1, Pallas kernels: 120 us -> 106 us  [whole_layer(): pl.pallas_call(partial(layer_kernel, depth), out_shape=jax.ShapeDtypeStru...]
where the time goes in v2:
time: 108 us
  Pallas kernels  106 us (98%)
  local copies, waits for them, and re-layouts  1.67 us (2%)
    pallas_call x1, Pallas kernels, whole_layer(): pl.pallas_call(partial(layer_kernel, depth), out_shape=jax.ShapeDtypeStru...  106 us

profile of v2, /device:TPU:0, one launch (start us, length us, event | category | flops | bytes accessed | tf_op | source)
XLA Modules:
  0.0 107.8 jit_solution(17745061626528745207)
XLA Ops:
  0.0 106.1 %shard_map.127 = bf16[64,2048]{1,0:T(8,128)(2,1)} custom-call(bf16[512,256]{1,0:T(8,128)(2,1)} %queries_hbm.1, bf16[512,256]{1,0:T(8,128)(2,1)} %keys_hbm.1, bf16[512,256]{1,0:T(8,128)(2,1)} %values_hbm.1, f32[2,512]{1,0:T(2,128)} %bitcast.8, f32[1,256]{1,0:T(1,128)} %bitcast.9, bf16[64,2048]{1,0:T(8,128)(2,1)} %stream_hbm.1, ...), custom_call_target="tpu_custom_call" | custom-call | tf_op jit(solution)/shard_map/pallas_call | solution.py:740
  106.1 1.7 %copy.15 = bf16[64,2048]{1,0:T(8,128)(2,1)} copy(bf16[64,2048]{1,0:T(8,128)(2,1)} %shard_map.127) | data formatting | bytes 524288

commit v3 on v2

--- a/solution.py
+++ b/solution.py
@@ -150,8 +150,7 @@
     norm_gain,
     routing,
     route_w,
-    key_all,
-    value_all,
+    pair_all,
     gate_all,
     weights_all,
     wcols,
@@ -182,9 +181,9 @@
     out_recv_sems,
     w_send_sems,
     w_recv_sems,
-    wq_recv_sems,
     ag_send_sems,
     ag_recv_sems,
+    part_recv_sems,
     rs_send_sems,
     core_sems,
     second_sems,
@@ -249,8 +248,8 @@
 
     load("gates", gates_hbm, gate_all.at[sp])
     for head in range(heads):
-        load(("keys", head), keys_hbm.at[:, head_cols(head)], key_all.at[sp, head])
-        load(("values", head), values_hbm.at[:, head_cols(head)], value_all.at[sp, head])
+        load(("keys", head), keys_hbm.at[:, head_cols(head)], pair_all.at[sp, head, 0])
+        load(("values", head), values_hbm.at[:, head_cols(head)], pair_all.at[sp, head, 1])
     load("queries", queries_hbm, queries)
     load("routing", routing_hbm, routing)
     load("route", route_hbm, route_w)
@@ -262,7 +261,7 @@
         pl.semaphore_signal(barrier, inc=1, device_id=peer, device_id_type=MESH)
     pl.semaphore_wait(barrier, len(peers))
 
-    sent = []
+    drains = []
 
     def send(src, dst, send_sem, recv_sem, target, when=None):
         copy = pltpu.make_async_remote_copy(
@@ -277,7 +276,9 @@
             copy.start()
         else:
             pl.when(when)(copy.start)
-        sent.append((copy, when))
+
+    def drain_later(ref, sem, when=None):
+        drains.append((ref, sem, when))
 
     def landed(dst, sem):
         pltpu.make_async_remote_copy(
@@ -289,28 +290,28 @@
             device_id_type=MESH,
         ).wait_recv()
 
-    def kv_refs(quad, head):
-        refs = [(key_all.at[quad, head], 2 * head), (value_all.at[quad, head], 2 * head + 1)]
-        return refs if head else [(gate_all.at[quad], 2 * heads)] + refs
-
-    kv_count = [0]
-
-    def kv_send(quad, head, target):
-        for ref, part in kv_refs(quad, head):
-            send(ref, ref, kv_send_sems.at[kv_count[0]], kv_recv_sems.at[quad, part], target)
-            kv_count[0] += 1
+    def kv_send(quad, head, target, lane):
+        if head == 0:
+            ref = gate_all.at[quad]
+            send(ref, ref, kv_send_sems.at[2], kv_recv_sems.at[quad, heads], target)
+        for ref in (pair_all.at[quad, head, 0], pair_all.at[quad, head, 1]):
+            send(ref, ref, kv_send_sems.at[lane], kv_recv_sems.at[quad, head], target)
 
     def kv_landed(quad, head):
-        for ref, part in kv_refs(quad, head):
-            landed(ref, kv_recv_sems.at[quad, part])
-
+        if head == 0:
+            landed(gate_all.at[quad], kv_recv_sems.at[quad, heads])
+        landed(pair_all.at[quad, head], kv_recv_sems.at[quad, head])
+
+    drain_later(pair_all.at[0], kv_send_sems.at[0])
+    drain_later(pair_all.at[0:2], kv_send_sems.at[1])
+    drain_later(gate_all.at[0:3], kv_send_sems.at[2])
     loads["gates"].wait()
     for head in range(heads):
         loads["keys", head].wait()
         loads["values", head].wait()
-        kv_send(sp, head, to_first)
+        kv_send(sp, head, to_first, 0)
         if head == 0:
-            kv_send(sp, head, to_second)
+            kv_send(sp, head, to_second, 1)
     load("stream", stream_hbm, stream)
     load("gain", gain_hbm, gain)
     load("norm", norm_hbm, norm_gain)
@@ -346,7 +347,7 @@
             rows = pl.ds(pl.multiple_of(j * chunk, chunk), chunk)
             scores = lax.dot_general(
                 queries[rows, cols],
-                key_all[quad, head],
+                pair_all[quad, head, 0],
                 (((1,), (1,)), ((), ())),
                 preferred_element_type=jnp.float32,
             )
@@ -365,7 +366,7 @@
             added = jnp.sum(lifted, axis=1, keepdims=True)
             product = jnp.dot(
                 lifted.astype(jnp.bfloat16),
-                value_all[quad, head],
+                pair_all[quad, head, 1],
                 preferred_element_type=jnp.float32,
             )
             if not diagonal:
@@ -390,28 +391,27 @@
 
     def take_first(head):
         kv_landed(first, head)
-        kv_send(first, head, to_second)
+        kv_send(first, head, to_second, 1)
         if head + 1 < heads:
-            kv_send(sp, head + 1, to_second)
+            kv_send(sp, head + 1, to_second, 1)
         attend_earlier(first, head)
 
     def take_second(head):
         kv_landed(second, head)
         attend_earlier(second, head)
 
-    out_count = [0]
-
     def finish(head):
         kv_landed(far, head)
         attend_earlier(far, head)
 
-        @pl.loop(0, tp_count)
-        def _(j):
-            rows = pl.ds(pl.multiple_of(j * count, count), count)
-            attended = weighted[head, rows] / weight_total[head, rows]
+        span = tokens // 2 if tp_count % 2 == 0 else tokens
+        for at in range(tokens // span):
+            rows = pl.ds(at * span, span)
+            attended = weighted[head, rows] * (1.0 / weight_total[head, rows])
             square = jnp.mean(attended * attended, axis=1, keepdims=True)
             normed = attended * lax.rsqrt(square + 1e-06) * gain[0:1, head_cols(head)]
-            leaving[head, j] = normed.astype(jnp.bfloat16)
+            blocks = span // count
+            leaving[head, pl.ds(at * blocks, blocks)] = bf16(normed).reshape(blocks, count, HD)
 
         for level in reversed(levels):
             for side in (core, other):
@@ -421,11 +421,11 @@
                 send(
                     leaving.at[head, target],
                     incoming.at[head, tp],
-                    out_send_sems.at[out_count[0]],
-                    out_recv_sems.at[head, tp],
+                    out_send_sems.at[head],
+                    out_recv_sems.at[head, z],
                     (sp, target),
                 )
-                out_count[0] += 1
+        drain_later(leaving.at[head, 0 : tp_count - 1], out_send_sems.at[head])
         incoming[head, tp] = leaving[head, tp]
 
     z_level = levels[0]
@@ -434,7 +434,8 @@
     for step in range(1, tp_count):
         target = (tp + step) % tp_count
         ref = weights_all.at[sp, tp]
-        send(ref, ref, w_send_sems.at[step], w_recv_sems.at[tp], (sp, target))
+        send(ref, ref, w_send_sems.at[0], w_recv_sems.at[QUADS], (sp, target))
+    drain_later(weights_all.at[0, 0 : tp_count - 1], w_send_sems.at[0])
     loads["gain"].wait()
     take_first(0)
     take_second(0)
@@ -444,38 +445,27 @@
         finish(head)
         if head + 1 < heads:
             take_second(head + 1)
-    for step in range(1, tp_count):
-        source = (tp + step) % tp_count
-        landed(weights_all.at[sp, source], w_recv_sems.at[source])
-
-    send(weights_all.at[sp], weights_all.at[sp], w_send_sems.at[0], wq_recv_sems.at[sp], to_first)
-    send(
-        weights_all.at[sp],
-        weights_all.at[sp],
-        w_send_sems.at[tp_count],
-        wq_recv_sems.at[sp],
-        to_second,
-    )
+    landed(weights_all.at[sp, 0 : tp_count - 1], w_recv_sems.at[QUADS])
+
+    def spread_weights(quad, target):
+        ref = weights_all.at[quad]
+        send(ref, ref, w_send_sems.at[1], w_recv_sems.at[quad], target)
+
+    spread_weights(sp, to_first)
+    spread_weights(sp, to_second)
+    drain_later(weights_all.at[0:3], w_send_sems.at[1])
     loads["stream"].wait()
     resid[...] = f32(stream[...])
     loads["norm"].wait()
-    landed(weights_all.at[first], wq_recv_sems.at[first])
-    send(
-        weights_all.at[first],
-        weights_all.at[first],
-        w_send_sems.at[tp_count + 1],
-        wq_recv_sems.at[first],
-        to_second,
-    )
-    strip = 512 if width % 512 == 0 else width
+    strip = 1024 if width % 1024 == 0 else width
     for head in range(heads):
         loads["out", head].wait()
         for level in levels:
             sources = (level * 2, level * 2 + 1)
-            for side in (core, other):
-                source = level * 2 + side
-                if not (level is z_level and side is core):
-                    landed(incoming.at[head, source], out_recv_sems.at[head, source])
+            from_level = incoming.at[head, pl.ds(level * 2, 2)]
+            if level is z_level:
+                from_level = incoming.at[head, level * 2 + other]
+            landed(from_level, out_recv_sems.at[head, level])
 
             @pl.loop(0, width // strip)
             def _(j, head=head, level=level, sources=sources):
@@ -484,6 +474,8 @@
                 weights = out_w[head, pl.ds(level * 2, 2), :, cols].reshape(2 * HD, strip)
                 resid[:, cols] += jnp.dot(rows, weights, preferred_element_type=jnp.float32)
 
+    landed(weights_all.at[first], w_recv_sems.at[first])
+    spread_weights(first, to_second)
     total = resid[...]
     center = total - jnp.mean(total, axis=1, keepdims=True)
     variance = jnp.mean(center * center, axis=1, keepdims=True)
@@ -491,30 +483,53 @@
         jnp.bfloat16
     )
 
-    ag_count = [0]
+    ag_count = [3]
 
     def part_of(k):
         return pl.ds(k * part_rows, part_rows)
 
-    def spread(level, quad, k, target, when=None):
+    def spread(level, quad, k, target, sem, recv_sem=None):
         ref = rows_all.at[core, level, quad, part_of(k)]
-        sem = ag_recv_sems.at[core, level, quad, k]
-        send(ref, ref, ag_send_sems.at[ag_count[0]], sem, target, when)
+        if recv_sem is None:
+            recv_sem = ag_recv_sems.at[level, quad, k]
+        send(ref, ref, ag_send_sems.at[sem], recv_sem, target)
+
+    def spread_all(level, quad, target, sem):
+        for k in range(PARTS):
+            spread(level, quad, k, target, sem)
+
+    def to_partner(level, quad, k):
+        spread(level, quad, k, to_core, 0, part_recv_sems.at[level])
+
+    def lane_when(when):
+        sem = ag_count[0]
         ag_count[0] += 1
-
-    def arrived(half, level, quad, k):
-        ref = rows_all.at[half, level, quad, part_of(k)]
-        landed(ref, ag_recv_sems.at[half, level, quad, k])
-
+        drain_later(rows_all.at[0, 0, 0], ag_send_sems.at[sem], when)
+
+        def spread_when(level, quad, k, target):
+            @pl.when(when)
+            def _():
+                spread(level, quad, k, target, sem)
+
+        return spread_when
+
+    def arrived(level, quad, k):
+        landed(rows_all.at[core, level, quad, part_of(k)], ag_recv_sems.at[level, quad, k])
+
+    drain_later(rows_all.at[0], ag_send_sems.at[0])
+    drain_later(rows_all.at[0, 0:2], ag_send_sems.at[1])
+    drain_later(rows_all.at[0, 0, 0], ag_send_sems.at[2])
     above, below = at_z((z + 1) % depth), at_z((z + depth - 1) % depth)
+    own_above, own_below = lane_when(z < depth - 1), lane_when(z > 0)
     for k in range(PARTS):
-        spread(z, sp, k, above, z < depth - 1)
-        spread(z, sp, k, below, z > 0)
-        for target in (to_first, to_second, to_core):
-            spread(z, sp, k, target)
-
-    landed(weights_all.at[second], wq_recv_sems.at[second])
-    landed(weights_all.at[far], wq_recv_sems.at[far])
+        own_above(z, sp, k, above)
+        own_below(z, sp, k, below)
+        spread(z, sp, k, to_first, 2)
+        spread(z, sp, k, to_second, 1)
+        to_partner(z, sp, k)
+
+    landed(weights_all.at[second], w_recv_sems.at[second])
+    landed(weights_all.at[far], w_recv_sems.at[far])
     lane = lax.broadcasted_iota(jnp.int32, (QUADS, LANES), 0)
     picked = []
     for quad in range(QUADS):
@@ -552,41 +567,48 @@
             product = jnp.dot(hidden[half, level], down_w[:, cols], preferred_element_type=jnp.float32)
             dest[level, :, :, cols] = bf16(product * weight).reshape(QUADS, count, piece)
 
-    rs_count = [0]
-
-    def send_back(src, dst, sem, target, when=None):
-        send(src, dst, rs_send_sems.at[rs_count[0]], sem, target, when)
-        rs_count[0] += 1
-
     def from_z_near(place):
         level = levels[place]
+        go_above = lane_when((level < z) & (z < depth - 1))
+        go_below = lane_when((level > z) & (z > 0))
+        go_first = lane_when((level - z) * (level - z) != 1)
         for k in range(PARTS):
-            arrived(core, level, sp, k)
-            spread(level, sp, k, above, (level < z) & (z < depth - 1))
-            spread(level, sp, k, below, (level > z) & (z > 0))
-            spread(level, sp, k, to_first, (level - z) * (level - z) != 1)
-            spread(level, sp, k, to_second)
-            spread(level, sp, k, to_core)
+            arrived(level, sp, k)
+            go_above(level, sp, k, above)
+            go_below(level, sp, k, below)
+            go_first(level, sp, k, to_first)
+            spread(level, sp, k, to_second, 1)
+            to_partner(level, sp, k)
 
     def from_first_near(place):
         level = levels[place]
+        if place == 0:
+            go_above, go_below = lane_when(z < depth - 1), lane_when(z > 0)
         for k in range(PARTS):
-            arrived(core, level, first, k)
+            arrived(level, first, k)
             if place == 0:
-                spread(level, first, k, above, z < depth - 1)
-                spread(level, first, k, below, z > 0)
-            spread(level, first, k, to_second)
-            spread(level, first, k, to_core)
+                go_above(level, first, k, above)
+                go_below(level, first, k, below)
+            spread(level, first, k, to_second, 1)
+            to_partner(level, first, k)
 
     def from_second_near(place):
         for k in range(PARTS):
-            arrived(core, levels[place], second, k)
-            spread(levels[place], second, k, to_core)
+            arrived(levels[place], second, k)
+            to_partner(levels[place], second, k)
 
     def from_far(place):
         for k in range(PARTS):
-            arrived(core, levels[place], far, k)
-            spread(levels[place], far, k, to_core)
+            arrived(levels[place], far, k)
+            to_partner(levels[place], far, k)
+
+    def send_back(src, dst, lane, sem, target, when=None):
+        send(src, dst, rs_send_sems.at[lane], sem, target, when)
+
+    drain_later(mine, rs_send_sems.at[0])
+    drain_later(rows_all.at[0, 0:2], rs_send_sems.at[1])
+    drain_later(rows_all.at[0, 0, 0:3], rs_send_sems.at[2])
+    drain_later(rows_all.at[0, 0, 0], rs_send_sems.at[3])
 
     def own_hidden(place):
         hidden_units(core, levels[place])
@@ -596,15 +618,13 @@
 
     def partner_hidden(place):
         level = levels[place]
-        for quad in range(QUADS):
-            for k in range(PARTS):
-                arrived(other, level, quad, k)
+        landed(rows_all.at[other, level], part_recv_sems.at[level])
         hidden_units(other, level)
 
     def partner_product(place):
         level = levels[place]
         down_product(other, level, theirs)
-        send_back(theirs.at[level], from_core.at[level], core_sems.at[level], to_core)
+        send_back(theirs.at[level], from_core.at[level], 0, core_sems.at[level], to_core)
 
     def both_halves(place):
         level = levels[place]
@@ -618,6 +638,7 @@
                 send_back(
                     mine.at[level, quad, rows],
                     from_second.at[level, slot, rows],
+                    1,
                     second_sems.at[level, slot, k],
                     to_second,
                 )
@@ -634,6 +655,10 @@
                         landed(from_zf.at[near, rows], zf_sems.at[near, k])
                     mine[z, first] = bf16(f32(mine[z, first]) + f32(from_zf[near]))
 
+        near, apart = adjacent(level), (level - z) * (level - z) != 1
+        if place:
+            drain_later(rows_all.at[0, 0, 0], rs_send_sems.at[2 + 2 * place], near)
+            drain_later(rows_all.at[0, 0, 0], rs_send_sems.at[3 + 2 * place], apart)
         for k in range(PARTS):
             rows = part_of(k)
             landed(from_second.at[level, 1, rows], second_sems.at[level, 1, k])
@@ -645,11 +670,11 @@
             src = mine.at[level, first, rows]
             dst, sem = from_first.at[level, rows], first_sems.at[level, k]
             if place:
-                near = adjacent(level)
-                send_back(src, from_zf.at[z, rows], zf_sems.at[z, k], at_z(level), near)
-                send_back(src, dst, sem, to_first, (level - z) * (level - z) != 1)
+                zf_dst, zf_sem = from_zf.at[z, rows], zf_sems.at[z, k]
+                send_back(src, zf_dst, 2 + 2 * place, zf_sem, at_z(level), near)
+                send_back(src, dst, 3 + 2 * place, sem, to_first, apart)
             else:
-                send_back(src, dst, sem, to_first)
+                send_back(src, dst, 3, sem, to_first)
 
     def onto_owner(place):
         level = levels[place]
@@ -677,7 +702,7 @@
                 mine[level, sp, rows] = bf16(total_of(False))
 
             src = mine.at[level, sp, rows]
-            send_back(src, from_z.at[z, rows], z_sems.at[z, k], at_z(level))
+            send_back(src, from_z.at[z, rows], 2, z_sems.at[z, k], at_z(level))
 
     tasks = dict(
         zr=from_z_near,
@@ -701,11 +726,22 @@
             landed(from_z.at[near, part_of(k)], z_sems.at[near, k])
         total = total + f32(from_z[near])
     out_ref[...] = total.astype(out_ref.dtype)
-    for copy, when in sent:
+
+    def drain(ref, sem):
+        pltpu.make_async_remote_copy(
+            src_ref=ref,
+            dst_ref=ref,
+            send_sem=sem,
+            recv_sem=kv_recv_sems.at[0, 0],
+            device_id=to_core,
+            device_id_type=MESH,
+        ).wait_send()
+
+    for ref, sem, when in drains:
         if when is None:
-            copy.wait_send()
+            drain(ref, sem)
         else:
-            pl.when(when)(copy.wait_send)
+            pl.when(when)(partial(drain, ref, sem))
 
 
 def whole_layer(
@@ -735,8 +771,6 @@
     vmem = pltpu.VMEM
     plane = (depth, QUADS, count, width)
     hbm = pl.BlockSpec(memory_space=pltpu.HBM)
-    ag_sends = PARTS * (5 + 5 * (depth - 1) + 2 * depth + 2 + 2 * depth)
-    rs_sends = depth + PARTS * (2 * depth + 2 * depth + depth)
     return pl.pallas_call(
         partial(layer_kernel, depth),
         out_shape=jax.ShapeDtypeStruct((count, width), bf16),
@@ -749,8 +783,7 @@
             vmem((1, width), f32),
             vmem((top, count), jnp.int32),
             vmem((top, count), f32),
-            vmem((QUADS, heads, tokens, HD), bf16),
-            vmem((QUADS, heads, tokens, HD), bf16),
+            vmem((QUADS, heads, 2, tokens, HD), bf16),
             vmem((QUADS, heads, tokens), f32),
             vmem((QUADS, tp_count, QUADS, LANES), f32),
             vmem((2, depth, QUADS, count, 1), f32),
@@ -775,16 +808,16 @@
             vmem((depth, count, width), bf16),
             vmem((depth, count, width), bf16),
             dma((10 + 3 * heads,)),
-            dma((3 + 6 * heads,)),
-            dma((QUADS, 1 + 2 * heads)),
-            dma((heads * (tp_count - 1),)),
-            dma((heads, tp_count)),
-            dma((tp_count + 2,)),
-            dma((tp_count,)),
-            dma((QUADS,)),
-            dma((ag_sends,)),
-            dma((2, depth, QUADS, PARTS)),
-            dma((rs_sends,)),
+            dma((3,)),
+            dma((QUADS, heads + 1)),
+            dma((heads,)),
+            dma((heads, depth)),
+            dma((2,)),
+            dma((QUADS + 1,)),
+            dma((3 + 2 + 2 + 3 * (depth - 1),)),
+            dma((depth, QUADS, PARTS)),
+            dma((depth,)),
+            dma((2 + 2 * depth,)),
             dma((depth,)),
             dma((depth, 2, PARTS)),
             dma((depth, PARTS)),
@@ -792,22 +825,27 @@
             dma((depth, PARTS)),
         ],
         compiler_params=pltpu.CompilerParams(
-            collective_id=0, has_side_effects=True, vmem_limit_bytes=58 * 2**20
+            collective_id=0, has_side_effects=True, vmem_limit_bytes=50 * 2**20
         ),
     )(
-        queries,
-        keys,
-        values,
-        jnp.transpose(forget_totals),
-        head_gain.reshape(1, -1),
-        stream,
-        out_weight.reshape(tp_count, heads, HD, width),
-        norm_gain.reshape(1, -1),
-        jnp.transpose(routing),
-        jnp.transpose(route_weights),
-        gate_weight,
-        up_weight,
-        down_weight,
+        *(
+            pltpu.with_memory_space_constraint(operand, pltpu.HBM)
+            for operand in (
+                queries,
+                keys,
+                values,
+                jnp.transpose(forget_totals),
+                head_gain.reshape(1, -1),
+                stream,
+                out_weight.reshape(tp_count, heads, HD, width),
+                norm_gain.reshape(1, -1),
+                jnp.transpose(routing),
+                jnp.transpose(route_weights),
+                gate_weight,
+                up_weight,
+                down_weight,
+            )
+        )
     )
 
 

time: 108 us -> 102 us (0.944)
  Pallas kernels: 106 us -> 102 us
    pallas_call x1, Pallas kernels: 106 us -> 102 us  [whole_layer(): pl.pallas_call(partial(layer_kernel, depth), out_shape=jax.ShapeDtypeStru...]
where the time goes in v3:
time: 102 us
  Pallas kernels  102 us (100%)
    pallas_call x1, Pallas kernels, whole_layer(): pl.pallas_call(partial(layer_kernel, depth), out_shape=jax.ShapeDtypeStru...  102 us

profile of v3, /device:TPU:0, one launch (start us, length us, event | category | flops | bytes accessed | tf_op | source)
XLA Modules:
  0.0 102.3 jit_solution(9398550434364088827)
XLA Ops:
  0.0 101.6 %shard_map.127 = bf16[64,2048]{1,0:T(8,128)(2,1)S(1)} custom-call(bf16[512,256]{1,0:T(8,128)(2,1)} %queries_hbm.1, bf16[512,256]{1,0:T(8,128)(2,1)} %keys_hbm.1, bf16[512,256]{1,0:T(8,128)(2,1)} %values_hbm.1, f32[2,512]{1,0:T(2,128)} %bitcast.8, f32[1,256]{1,0:T(1,128)} %bitcast.9, bf16[64,2048]{1,0:T(8,128)(2,1)} %stream_hbm.1, ...), custom_call_target="tpu_custom_call" | custom-call | tf_op jit(solution)/shard_map/pallas_call | solution.py:774
  101.6 0.7 copy.15

commit v4 on v3

--- a/solution.py
+++ b/solution.py
@@ -174,6 +174,7 @@
     from_first,
     from_z,
     from_zf,
+    word_sems,
     local_sems,
     kv_send_sems,
     kv_recv_sems,
@@ -255,11 +256,39 @@
     load("route", route_hbm, route_w)
 
     barrier = pltpu.get_barrier_semaphore()
-    peers = [to_first, to_second]
-    peers += [(sp, (tp + step) % tp_count) for step in range(1, tp_count)]
-    for peer in peers:
+    inner = z * (depth - 1 - z)
+    above, below = at_z((z + 1) % depth), at_z((z + depth - 1) % depth)
+
+    def greet(sems):
+        sides = ((None, to_core, 0), (z < depth - 1, above, 1), (z > 0, below, 2))
+        for when, peer, side in sides:
+
+            def signal(peer=peer, side=side):
+                pl.semaphore_signal(sems(side), inc=1, device_id=peer, device_id_type=MESH)
+
+            if when is None:
+                signal()
+            else:
+                pl.when(when)(signal)
+
+    for peer in (to_first, to_second):
         pl.semaphore_signal(barrier, inc=1, device_id=peer, device_id_type=MESH)
-    pl.semaphore_wait(barrier, len(peers))
+    greet(lambda side: barrier)
+    pl.semaphore_wait(barrier, 5 - 1 // (1 + inner))
+
+    def word(stage):
+        greet(lambda side: word_sems.at[stage, side])
+
+    def hear(stage):
+        for when, side in ((None, 0), (z > 0, 1), (z < depth - 1, 2)):
+
+            def listen(side=side):
+                pl.semaphore_wait(word_sems.at[stage, side], 1)
+
+            if when is None:
+                listen()
+            else:
+                pl.when(when)(listen)
 
     drains = []
 
@@ -340,11 +369,14 @@
             row = gate_all[sp, head : head + 1, span] * LOG2E
             qcol[head, span] = jnp.transpose(jnp.broadcast_to(row, (chunk, chunk)))[:, :1]
 
-    def attend(quad, head, diagonal):
+    halves = 2 if tokens % (2 * chunk) == 0 and tp_count % 2 == 0 else 1
+
+    def attend(quad, head, diagonal, parts):
         cols = head_cols(head)
 
         def attend_chunk(j):
-            rows = pl.ds(pl.multiple_of(j * chunk, chunk), chunk)
+            start = j * chunk
+            rows = pl.ds(start if isinstance(start, int) else pl.multiple_of(start, chunk), chunk)
             scores = lax.dot_general(
                 queries[rows, cols],
                 pair_all[quad, head, 0],
@@ -355,7 +387,7 @@
             key_gate = gate_all[quad, head : head + 1, :] * LOG2E
             scores = scores * (HD ** (-0.5) * LOG2E) - key_gate
             if diagonal:
-                row_id = lax.broadcasted_iota(jnp.int32, scores.shape, 0) + j * chunk
+                row_id = lax.broadcasted_iota(jnp.int32, scores.shape, 0) + start
                 col_id = lax.broadcasted_iota(jnp.int32, scores.shape, 1)
                 scores = jnp.where(col_id <= row_id, scores, masked_score)
             new_peak = jnp.max(scores, axis=1, keepdims=True) + query_gate
@@ -373,21 +405,23 @@
                 rescale = jnp.exp2(old_peak - new_peak)
                 added = weight_total[head, rows] * rescale + added
                 product = weighted[head, rows] * rescale + product
-            peak[head, rows] = new_peak
-            weight_total[head, rows] = added
-            weighted[head, rows] = product
-
-        pairs = 2 if tokens % (2 * chunk) == 0 else 1
-
-        @pl.loop(0, tokens // (pairs * chunk))
-        def _(j):
-            for at in range(pairs):
-                attend_chunk(j * pairs + at)
-
-    def attend_earlier(quad, head):
+            return rows, new_peak, added, product
+
+        group = tokens // (halves * chunk)
+
+        def attend_group(j):
+            for rows, new_peak, added, product in [attend_chunk(j * group + at) for at in range(group)]:
+                peak[head, rows] = new_peak
+                weight_total[head, rows] = added
+                weighted[head, rows] = product
+
+        for part in parts:
+            attend_group(part)
+
+    def attend_earlier(quad, head, parts=tuple(range(halves))):
         @pl.when(quad < sp)
         def _():
-            attend(quad, head, False)
+            attend(quad, head, False, parts)
 
     def take_first(head):
         kv_landed(first, head)
@@ -402,35 +436,38 @@
 
     def finish(head):
         kv_landed(far, head)
-        attend_earlier(far, head)
-
-        span = tokens // 2 if tp_count % 2 == 0 else tokens
-        for at in range(tokens // span):
-            rows = pl.ds(at * span, span)
+        span, blocks = tokens // halves, tp_count // halves
+        for part in range(halves):
+            attend_earlier(far, head, (part,))
+            rows = pl.ds(part * span, span)
             attended = weighted[head, rows] * (1.0 / weight_total[head, rows])
             square = jnp.mean(attended * attended, axis=1, keepdims=True)
             normed = attended * lax.rsqrt(square + 1e-06) * gain[0:1, head_cols(head)]
-            blocks = span // count
-            leaving[head, pl.ds(at * blocks, blocks)] = bf16(normed).reshape(blocks, count, HD)
-
-        for level in reversed(levels):
-            for side in (core, other):
-                if level is z_level and side is core:
-                    continue
-                target = level * 2 + side
-                send(
-                    leaving.at[head, target],
-                    incoming.at[head, tp],
-                    out_send_sems.at[head],
-                    out_recv_sems.at[head, z],
-                    (sp, target),
-                )
+            targets = range(part * blocks, (part + 1) * blocks)
+            leaving[head, targets.start : targets.stop] = bf16(normed).reshape(blocks, count, HD)
+            for target in targets:
+
+                @pl.when(tp != target)
+                def _(target=target):
+                    send(
+                        leaving.at[head, target],
+                        incoming.at[head, tp],
+                        out_send_sems.at[head],
+                        out_recv_sems.at[head, z],
+                        (sp, target),
+                    )
+
         drain_later(leaving.at[head, 0 : tp_count - 1], out_send_sems.at[head])
         incoming[head, tp] = leaving[head, tp]
 
     z_level = levels[0]
+    word(0)
     for head in range(heads):
-        attend(sp, head, True)
+        attend(sp, head, True, range(halves))
+    for stage in range(depth - 1):
+        hear(stage)
+        if stage + 1 < depth - 1:
+            word(stage + 1)
     for step in range(1, tp_count):
         target = (tp + step) % tp_count
         ref = weights_all.at[sp, tp]
@@ -519,7 +556,6 @@
     drain_later(rows_all.at[0], ag_send_sems.at[0])
     drain_later(rows_all.at[0, 0:2], ag_send_sems.at[1])
     drain_later(rows_all.at[0, 0, 0], ag_send_sems.at[2])
-    above, below = at_z((z + 1) % depth), at_z((z + depth - 1) % depth)
     own_above, own_below = lane_when(z < depth - 1), lane_when(z > 0)
     for k in range(PARTS):
         own_above(z, sp, k, above)
@@ -807,6 +843,7 @@
             vmem((depth, count, width), bf16),
             vmem((depth, count, width), bf16),
             vmem((depth, count, width), bf16),
+            pltpu.SemaphoreType.REGULAR((depth - 1, 3)),
             dma((10 + 3 * heads,)),
             dma((3,)),
             dma((QUADS, heads + 1)),

time: 102 us -> 99.9 us (0.979)
  Pallas kernels: 102 us -> 99.1 us
    pallas_call x1, Pallas kernels: 102 us -> 99.1 us  [whole_layer(): pl.pallas_call(partial(layer_kernel, depth), out_shape=jax.ShapeDtypeStru...]
where the time goes in v4:
time: 99.9 us; the launch traced here: 99.8 us
  Pallas kernels  99.1 us (99%)
    pallas_call x1, Pallas kernels, whole_layer(): pl.pallas_call(partial(layer_kernel, depth), out_shape=jax.ShapeDtypeStru...  99.1 us

profile of v4, /device:TPU:0, one launch (start us, length us, event | category | flops | bytes accessed | tf_op | source)
XLA Modules:
  0.0 99.8 jit_solution(13660921005601690826)
XLA Ops:
  0.0 99.1 %shard_map.127 = bf16[64,2048]{1,0:T(8,128)(2,1)S(1)} custom-call(bf16[512,256]{1,0:T(8,128)(2,1)} %queries_hbm.1, bf16[512,256]{1,0:T(8,128)(2,1)} %keys_hbm.1, bf16[512,256]{1,0:T(8,128)(2,1)} %values_hbm.1, f32[2,512]{1,0:T(2,128)} %bitcast.8, f32[1,256]{1,0:T(1,128)} %bitcast.9, bf16[64,2048]{1,0:T(8,128)(2,1)} %stream_hbm.1, ...), custom_call_target="tpu_custom_call" | custom-call | tf_op jit(solution)/shard_map/pallas_call | solution.py:810
  99.1 0.7 copy.15

commit v5 on v4

--- a/solution.py
+++ b/solution.py
@@ -84,43 +84,43 @@
 TASKS = (
     ("zr", 1),
     ("fa", 0),
+    ("s", 1),
     ("zr", 2),
     ("fa", 1),
-    ("s", 1),
     ("fa", 2),
-    ("d", 0),
-    ("s", 0),
-    ("co1", 0),
     ("zr", 3),
     ("d", 1),
-    ("s", 2),
     ("co1", 1),
     ("cp1", 1),
     ("d", 2),
     ("cp2", 1),
+    ("s", 2),
     ("fa", 3),
     ("co1", 2),
     ("co2", 1),
     ("r1", 1),
+    ("s", 3),
     ("cp1", 2),
+    ("cp2", 2),
+    ("r2", 1),
     ("d", 3),
-    ("cp2", 2),
-    ("s", 3),
-    ("r2", 1),
     ("co2", 2),
     ("r1", 2),
     ("cp1", 3),
     ("r3", 1),
+    ("d", 0),
+    ("cp2", 3),
+    ("s", 0),
+    ("r2", 2),
     ("co1", 3),
-    ("cp2", 3),
-    ("r2", 2),
-    ("co2", 0),
     ("co2", 3),
     ("r1", 3),
     ("r3", 2),
     ("cp1", 0),
     ("cp2", 0),
     ("r2", 3),
+    ("co1", 0),
+    ("co2", 0),
     ("r1", 0),
     ("r3", 3),
     ("r2", 0),

time: 99.9 us -> 100 us (level)
  no operation moved by 1% of the time
where the time goes in v5:
time: 100 us; the launch traced here: 99.8 us
  Pallas kernels  99.1 us (99%)
    pallas_call x1, Pallas kernels, whole_layer(): pl.pallas_call(partial(layer_kernel, depth), out_shape=jax.ShapeDtypeStru...  99.1 us

profile of v5, /device:TPU:0, one launch (start us, length us, event | category | flops | bytes accessed | tf_op | source)
XLA Modules:
  0.0 99.8 jit_solution(7141372277668778419)
XLA Ops:
  0.0 99.1 %shard_map.127 = bf16[64,2048]{1,0:T(8,128)(2,1)S(1)} custom-call(bf16[512,256]{1,0:T(8,128)(2,1)} %queries_hbm.1, bf16[512,256]{1,0:T(8,128)(2,1)} %keys_hbm.1, bf16[512,256]{1,0:T(8,128)(2,1)} %values_hbm.1, f32[2,512]{1,0:T(2,128)} %bitcast.8, f32[1,256]{1,0:T(1,128)} %bitcast.9, bf16[64,2048]{1,0:T(8,128)(2,1)} %stream_hbm.1, ...), custom_call_target="tpu_custom_call" | custom-call | tf_op jit(solution)/shard_map/pallas_call | solution.py:810
  99.1 0.7 copy.15
